TPU v7x, 32 devices: a whole 2x2x4 slice. The times are simulated.
32 devices in a mesh: grp: 2 (over x), ep: 16 (over z, y, core).
Axes of the slice: x: 2, y: 2, z: 4, core: 2. Of those that a mesh axis runs over, the one named last changes fastest.
Arguments:
- hidden: bfloat16 [4096, 2048], P(('grp', 'ep')), parts along dimension 0, may hold values from -6 to 6
- state: float32 [2, 4096, 4096], P(None, ('grp', 'ep')), parts along dimension 1, may hold values from -6 to 6
- norm_gain: float32 [2048], replicated, may hold values from 0.1 to 1.9
- w_in: bfloat16 [2048, 1024], P(None, 'ep'), may hold values from -0.125 to 0.125
- lam_re: float32 [64, 64], replicated, may hold values from -1 to -0.1
- lam_im: float32 [64, 64], replicated, may hold values from 0 to 200
- log_step: float32 [64], replicated, may hold values from -4.6 to -0.7
- in_re: float32 [64, 64, 16], replicated, may hold values from -1 to 1
- in_im: float32 [64, 64, 16], replicated, may hold values from -1 to 1
- out_re: float32 [64, 16, 64], replicated, may hold values from -0.75 to 0.75
- out_im: float32 [64, 16, 64], replicated, may hold values from -0.75 to 0.75
- skip: float32 [1024], replicated, may hold values from -4 to 4
- w_glu: bfloat16 [1024, 1024], replicated, may hold values from -0.1875 to 0.1875
- w_out: bfloat16 [1024, 2048], replicated, may hold values from -0.375 to 0.375
- ffn_gain: float32 [2048], replicated, may hold values from 0.1 to 1.9
- w_group: bfloat16 [2048, 4], replicated, may hold values from -0.03125 to 0.03125
- w_route: bfloat16 [2048, 16], replicated, may hold values from -0.03125 to 0.03125
- w_gate: bfloat16 [16, 2048, 512], P('ep'), may hold values from -0.125 to 0.125
- w_up: bfloat16 [16, 2048, 512], P('ep'), may hold values from -0.125 to 0.125
- w_down: bfloat16 [16, 512, 2048], P('ep'), may hold values from -2 to 2
- route_ids: int32 [4096, 2], P(('grp', 'ep')), parts along dimension 0, may hold values from 0 to 15, as said below
Outputs:
- hidden_out: bfloat16 [4096, 2048], P(('grp', 'ep')), parts along dimension 0
- new_state: float32 [2, 4096, 4096], P(None, ('grp', 'ep')), parts along dimension 1
There are 2 independent parts, one for each index of `grp`. A program takes and returns all parts, laid end to end along the dimension named above; an argument that names none is the same for every part. Nothing has to cross between parts.
Inputs may be any that keep to these rules, and one draw needn't show every extreme that they name: `route_ids`: each row names 2 different experts of one expert group (experts g * 4 to g * 4 + 3). Among the rows of one device no expert is named more than 32 times, and in every draw some experts are named exactly 32 times by the rows of every device.
All inputs are finite; a program needn't handle non-finite values.
Results may differ from a plain program's by a relative error of at most 0.013.
Values may be sent and summed in bfloat16 or wider, within the bound.
No kernel may reach another device: no remote copies, remote signals or barrier semaphores. Data moves between devices by JAX's collectives and lax.ppermute only.
A program may use at most 128 MiB of HBM per device.

v0:
```python
import jax
import jax.numpy as jnp
from jax import lax
from jax.sharding import PartitionSpec as P

EXP_GROUPS = 4
EXP_DEV = 1
TOPK = 2


def normalize(rows, gain):
    wide = rows.astype(jnp.float32)
    return wide * lax.rsqrt(jnp.mean(wide * wide, axis=-1, keepdims=True) + 1e-06) * gain


def discretize(lam_re, lam_im, log_step, in_re, in_im):
    step = jnp.exp(log_step)[:, None]
    magnitude = jnp.exp(lam_re * step)
    bar_re = magnitude * jnp.cos(lam_im * step)
    bar_im = magnitude * jnp.sin(lam_im * step)
    denom = lam_re * lam_re + lam_im * lam_im
    lessened = bar_re - 1.0
    coef_re = (lessened * lam_re + bar_im * lam_im) / denom
    coef_im = (bar_im * lam_re - lessened * lam_im) / denom
    drive_re = coef_re[:, :, None] * in_re - coef_im[:, :, None] * in_im
    drive_im = coef_re[:, :, None] * in_im + coef_im[:, :, None] * in_re
    return (bar_re, bar_im, drive_re, drive_im)


def mixer_step(inputs, state, lam_re, lam_im, log_step, in_re, in_im, out_re, out_im, skip, w_glu):
    rows = inputs.shape[0]
    groups, entries = lam_re.shape
    width = in_re.shape[2]
    highest = lax.Precision.HIGHEST
    bar_re, bar_im, drive_re, drive_im = discretize(lam_re, lam_im, log_step, in_re, in_im)
    wide = inputs.astype(jnp.float32)
    grouped = wide.reshape(rows, groups, width)
    push_re = jnp.einsum("bgc,gnc->bgn", grouped, drive_re, precision=highest)
    push_im = jnp.einsum("bgc,gnc->bgn", grouped, drive_im, precision=highest)
    old_re = state[0].reshape(rows, groups, entries)
    old_im = state[1].reshape(rows, groups, entries)
    new_re = bar_re * old_re - bar_im * old_im + push_re
    new_im = bar_re * old_im + bar_im * old_re + push_im
    read = jnp.einsum("bgn,gcn->bgc", new_re, out_re, precision=highest) - jnp.einsum(
        "bgn,gcn->bgc", new_im, out_im, precision=highest
    )
    mixed = read.reshape(rows, groups * width) + skip * wide
    active = jax.nn.gelu(mixed)
    gating = jnp.dot(active.astype(jnp.bfloat16), w_glu, preferred_element_type=jnp.float32)
    result = (active * jax.nn.sigmoid(gating)).astype(jnp.bfloat16)
    new_state = jnp.stack([new_re.reshape(rows, -1), new_im.reshape(rows, -1)])
    return (result, new_state)


def route_gates(normed, w_group, w_route, route_ids, per_group):
    group_logit = jnp.dot(normed, w_group, preferred_element_type=jnp.float32)
    route_logit = jnp.dot(normed, w_route, preferred_element_type=jnp.float32)
    chosen = route_ids[:, 0] // per_group
    pick_group = (
        chosen[:, None] == jnp.arange(group_logit.shape[1], dtype=jnp.int32)[None, :]
    ).astype(jnp.float32)
    own = jnp.sum(group_logit * pick_group, axis=1, keepdims=True)
    group_weight = 1.0 / jnp.sum(jnp.exp(group_logit - own), axis=1)
    pick = (
        route_ids[:, :, None] == jnp.arange(route_logit.shape[1], dtype=jnp.int32)[None, None, :]
    ).astype(jnp.float32)
    chosen_logit = jnp.sum(pick * route_logit[:, None, :], axis=2)
    first = jax.nn.sigmoid(chosen_logit[:, 0] - chosen_logit[:, 1])
    pair = jnp.stack([first, 1.0 - first], axis=1)
    return group_weight[:, None] * pair


def on_device(
    hidden,
    state,
    norm_gain,
    w_in,
    lam_re,
    lam_im,
    log_step,
    in_re,
    in_im,
    out_re,
    out_im,
    skip,
    w_glu,
    w_out,
    ffn_gain,
    w_group,
    w_route,
    w_gate,
    w_up,
    w_down,
    route_ids,
):
    normed = normalize(hidden, norm_gain).astype(jnp.bfloat16)
    inputs = jnp.dot(
        normed, lax.all_gather(w_in, "ep", axis=1, tiled=True), preferred_element_type=jnp.float32
    ).astype(jnp.bfloat16)
    glu, new_state = mixer_step(
        inputs, state, lam_re, lam_im, log_step, in_re, in_im, out_re, out_im, skip, w_glu
    )
    resid = (
        hidden.astype(jnp.float32) + jnp.dot(glu, w_out, preferred_element_type=jnp.float32)
    ).astype(jnp.bfloat16)
    normed2 = normalize(resid, ffn_gain).astype(jnp.bfloat16)
    experts = w_route.shape[1]
    gates = route_gates(normed2, w_group, w_route, route_ids, experts // EXP_GROUPS)
    count_dev = normed2.shape[0]
    model_width = normed2.shape[1]
    capacity = 2 * TOPK * count_dev // experts
    flat = route_ids.reshape(-1)
    hits = (flat[:, None] == jnp.arange(experts, dtype=jnp.int32)[None, :]).astype(jnp.int32)
    before = jnp.sum((jnp.cumsum(hits, axis=0) - hits) * hits, axis=1)
    slot = flat * capacity + before
    place = (slot[:, None] == jnp.arange(experts * capacity, dtype=jnp.int32)[None, :]).astype(
        jnp.bfloat16
    )
    dispatch = jnp.sum(place.reshape(count_dev, TOPK, experts * capacity), axis=1)
    outgoing = jnp.einsum("rs,rd->sd", dispatch, normed2, preferred_element_type=jnp.float32)
    outgoing = outgoing.astype(jnp.bfloat16).reshape(experts, capacity, model_width)
    sources = lax.axis_size("ep")
    received = lax.all_to_all(outgoing, "ep", split_axis=0, concat_axis=0, tiled=True)
    items = received.shape[1]
    arranged = received.reshape(sources, EXP_DEV, items, model_width).transpose(1, 0, 2, 3)
    arranged = arranged.reshape(EXP_DEV, sources * items, model_width)
    gate = jnp.einsum("erd,edf->erf", arranged, w_gate, preferred_element_type=jnp.float32)
    upper = jnp.einsum("erd,edf->erf", arranged, w_up, preferred_element_type=jnp.float32)
    inner = (jax.nn.silu(gate) * upper).astype(jnp.bfloat16)
    result = jnp.einsum("erf,efd->erd", inner, w_down, preferred_element_type=jnp.float32).astype(
        jnp.bfloat16
    )
    result = result.reshape(EXP_DEV, sources, items, model_width).transpose(1, 0, 2, 3)
    result = result.reshape(sources * EXP_DEV, items, model_width)
    returned = lax.all_to_all(result, "ep", split_axis=0, concat_axis=0, tiled=True)
    picked = returned.reshape(experts * capacity, model_width)[slot].reshape(
        count_dev, TOPK, model_width
    )
    moe = jnp.sum(picked.astype(jnp.float32) * gates[:, :, None], axis=1)
    hidden_out = (resid.astype(jnp.float32) + moe).astype(jnp.bfloat16)
    return (hidden_out, new_state)


def solution(mesh):
    return jax.shard_map(
        on_device,
        mesh=mesh,
        in_specs=(
            P(("grp", "ep"), None),
            P(None, ("grp", "ep"), None),
            P(),
            P(None, "ep"),
            P(),
            P(),
            P(),
            P(),
            P(),
            P(),
            P(),
            P(),
            P(),
            P(),
            P(),
            P(),
            P(),
            P("ep", None, None),
            P("ep", None, None),
            P("ep", None, None),
            P(("grp", "ep"), None),
        ),
        out_specs=(P(("grp", "ep"), None), P(None, ("grp", "ep"), None)),
        check_vma=False,
    )
```

profile of v0, /device:TPU:13, one launch (start us, length us, event | category | flops | bytes accessed | tf_op | source)
XLA Modules:
  0.0 221.1 jit_solution(17480860268676464589)
XLA Ops:
  7.2 0.0 copy-start
  7.2 0.0 all-gather.2.cloned.1.call-start
  7.2 0.7 all-gather.2.cloned.1.call-update
  7.9 0.8 copy.62
  8.7 0.1 eq.71
  8.8 0.1 eq.67
  9.0 0.7 exp.22
  9.7 0.6 reduce-window.6
  10.2 0.2 slice_reduce_fusion
  10.5 0.1 fusion.63
  10.6 0.1 reduce_sum.81
  10.7 0.6 broadcast_multiply_fusion
  11.3 0.1 copy.66
  11.4 4.7 %fusion.76 = (f32[1,128,4096]{2,1,0:T(8,128)}, f32[1,128,4096]{2,1,0:T(8,128)}) fusion(f32[2,128,4096]{2,1,0:T(8,128)} %param.22), kind=kLoop, calls=%fused_computation.103 | loop fusion | bytes 8388608 | tf_op jit(solution)/shard_map/slice | solution.py:40
  16.1 2.9 %copy.58 = f32[1,128,4096]{1,2,0:T(8,128)} copy(f32[1,128,4096]{2,1,0:T(8,128)} %get-tuple-element.4) | data formatting | bytes 4194304 | tf_op jit(solution)/shard_map/slice | solution.py:40
  19.1 3.0 %copy.59 = f32[1,128,4096]{1,2,0:T(8,128)} copy(f32[1,128,4096]{2,1,0:T(8,128)} %get-tuple-element.5) | data formatting | bytes 4194304 | tf_op jit(solution)/shard_map/slice | solution.py:41
  22.0 0.1 fusion.41
  22.2 0.2 fusion.18
  22.4 0.9 fusion.60
  23.3 38.0 %all-gather.2.cloned.1.call-done = bf16[2048,1024]{0,1:T(8,128)(2,1)} async-done(((bf16[2048,64]{0,1:T(8,128)(2,1)}), bf16[2048,1024]{0,1:T(8,128)(2,1)}) %all-gather.2.cloned.1.call-update) | async-done | bytes 4194320 | tf_op jit(solution)/shard_map/all_gather | solution.py:98
  61.2 4.4 %convolution_convert_fusion.2 = bf16[128,1024]{1,0:T(8,128)(2,1)} fusion(bf16[2048,1024]{0,1:T(8,128)(2,1)} %all-gather.2.cloned.1.call-done, bf16[128,2048]{1,0:T(8,128)(2,1)S(1)} %copy-done.6, f32[2048]{0:T(1024)S(1)} %copy-done.22, f32[128]{0:T(128)S(1)} %add_rsqrt_fusion.1), kind=kOutput, calls=%fused_computation.26 | convolution fusion | flops 538050560 | bytes 4989440 | tf_op jit(solution)/shard_map/dot_general | solution.py:97
  65.6 1.1 copy.60
  66.8 0.0 copy-start.4
  66.8 4.9 %bitcast_add_fusion = f32[128,64,64]{0,2,1:T(8,128)S(1)} fusion(f32[128,64,64]{0,2,1:T(8,128)} %bitcast.73, f32[128,64,64]{0,2,1:T(8,128)} %bitcast.75, bf16[128,64,16]{0,2,1:T(8,128)(2,1)S(1)} %bitcast.78, f32[64,64]{1,0:T(8,128)} %get-tuple-element.7, f32[64,64]{1,0:T(8,128)} %get-tuple-element.8, f32[64,64,16]{1,2,0:T(8,128)} %param.28, ...), kind=kOutput, calls=%fused_computation.12 | convolution fusion | flops 102957056 | bytes 7143424 | tf_op jit(solution)/shard_map/bgc,gnc->bgn/dot_general | solution.py:39
  71.8 3.2 %bitcast_add_fusion.1 = f32[128,64,64]{0,2,1:T(8,128)S(1)} fusion(f32[128,64,64]{0,2,1:T(8,128)S(1)} %bitcast.76, f32[128,64,64]{0,2,1:T(8,128)S(1)} %bitcast.74, bf16[128,64,16]{0,2,1:T(8,128)(2,1)S(1)} %bitcast.79, f32[64,64]{1,0:T(8,128)S(1)} %copy-done.14, f32[64,64]{1,0:T(8,128)S(1)} %copy-done.15, f32[64,64,16]{1,2,0:T(8,128)S(1)} %copy-done.8, ...), kind=kOutput, calls=%fused_computation.13 | convolution fusion | flops 102957056 | bytes 7143424 | tf_op jit(solution)/shard_map/bgc,gnc->bgn/dot_general | solution.py:38
  75.1 1.9 fusion.79
  77.0 1.9 convolution_subtract_fusion
  78.9 1.0 copy.61
  79.9 5.6 %multiply_reduce_fusion.1 = (f32[128]{0:T(128)S(1)}, f32[128,2048]{1,0:T(8,128)}) fusion(bf16[1024,2048]{1,0:T(8,128)(2,1)} %param.34, bf16[1024,1024]{1,0:T(8,128)(2,1)} %param.33, f32[128,1024]{1,0:T(8,128)} %copy.61, bf16[128,1024]{1,0:T(8,128)(2,1)S(1)} %copy-done.10, f32[1024]{0:T(1024)S(1)} %copy-done.26, bf16[128,2048]{1,0:T(8,128)(2,1)S(1)} %copy-done.6), kind=kOutput, calls=%fused_computation.32 | convolution fusion | flops 810549120 | bytes 8655360 | tf_op jit(solution)/shard_map/dot_general | solution.py:104
  85.6 1.4 multiply_convert_fusion
  87.0 0.7 convolution_convert_fusion
  87.7 51.6 %all_to_all.10 = bf16[16,32,2048]{2,1,0:T(8,128)(2,1)S(1)} all-to-all(bf16[16,32,2048]{2,1,0:T(8,128)(2,1)S(1)} %bitcast.77), channel_id=1, replica_groups=mesh['grp'=2,'ep'=16] {'ep'}, dimensions={0} | all-to-all | bytes 4194304 | tf_op jit(solution)/shard_map/all_to_all | solution.py:123
  139.3 1.3 copy-done.7
  140.7 2.2 %fusion.5 = f32[512,512]{1,0:T(8,128)} fusion(bf16[512,2048]{1,0:T(8,128)(2,1)S(1)} %bitcast.82, bf16[1,2048,512]{2,1,0:T(8,128)(2,1)S(1)} %copy-done.25), kind=kOutput, calls=%fused_computation.10 | convolution fusion | flops 1073741824 | bytes 5242880 | tf_op jit(solution)/shard_map/erd,edf->erf/dot_general | solution.py:127
  142.9 6.2 %convolution_convert_fusion.1 = bf16[512,2048]{1,0:T(8,128)(2,1)} fusion(bf16[1,512,2048]{2,1,0:T(8,128)(2,1)S(1)} %copy-done, bf16[512,2048]{1,0:T(8,128)(2,1)} %bitcast.83, bf16[1,2048,512]{2,1,0:T(8,128)(2,1)} %param.39, f32[512,512]{1,0:T(8,128)} %fusion.5), kind=kOutput, calls=%fused_computation.3 | convolution fusion | flops 2150105088 | bytes 9437184 | tf_op jit(solution)/shard_map/erf,efd->erd/dot_general | solution.py:130
  149.1 5.2 %all-to-all-start.1 = ((bf16[16,32,2048]{2,1,0:T(8,128)(2,1)}), bf16[16,32,2048]{2,1,0:T(8,128)(2,1)}, u32[]{:S(2)}, u32[]{:S(2)}) async-start(bf16[16,32,2048]{2,1,0:T(8,128)(2,1)} %bitcast.81), calls=%async_computation.1 | async-start | bytes 4194304 | tf_op jit(solution)/shard_map/all_to_all | solution.py:135
  154.3 0.1 mul.278
  154.5 0.3 select_reduce_fusion.1
  154.8 0.2 fusion.80
  155.1 0.1 copy.67
  155.2 2.9 %copy.69 = f32[1,128,4096]{2,1,0:T(8,128)} copy(f32[1,128,4096]{1,2,0:T(8,128)} %bitcast.72) | data formatting | bytes 4194304 | tf_op jit(solution)/shard_map/stack;reshape | solution.py:51
  158.2 2.9 %copy.68 = f32[1,128,4096]{2,1,0:T(8,128)} copy(f32[1,128,4096]{1,2,0:T(8,128)} %bitcast.71) | data formatting | bytes 4194304 | tf_op jit(solution)/shard_map/stack;reshape | solution.py:51
  161.1 4.7 %pad_maximum_fusion = f32[2,128,4096]{2,1,0:T(8,128)} fusion(f32[1,128,4096]{2,1,0:T(8,128)} %copy.69, f32[1,128,4096]{2,1,0:T(8,128)} %copy.68), kind=kLoop, calls=%fused_computation.1 | loop fusion | flops 1048576 | bytes 8388608 | tf_op jit(solution)/shard_map/stack | solution.py:51
  165.8 36.1 %all-to-all-done.1 = bf16[16,32,2048]{2,1,0:T(8,128)(2,1)} async-done(((bf16[16,32,2048]{2,1,0:T(8,128)(2,1)}), bf16[16,32,2048]{2,1,0:T(8,128)(2,1)}, u32[]{:S(2)}, u32[]{:S(2)}) %all-to-all-start.1) | async-done | bytes 2097184 | tf_op jit(solution)/shard_map/all_to_all | solution.py:135
  201.8 4.2 %gather_fusion = bf16[256,2048]{1,0:T(8,128)(2,1)S(1)} fusion(bf16[512,2048]{1,0:T(8,128)(2,1)} %bitcast.14, s32[1024]{0:T(1024)S(1)} %pad_clamp_fusion), kind=kCustom, calls=%fused_computation | custom fusion | bytes 2098176 | tf_op jit(solution)/shard_map/gather | solution.py:136
  206.1 2.4 %reshape.176 = f32[128,2,2048]{2,1,0:T(2,128)} reshape(bf16[256,2048]{1,0:T(8,128)(2,1)S(1)} %gather_fusion) | data formatting | bytes 3145728 | tf_op jit(solution)/shard_map/convert_element_type | solution.py:139
  208.4 4.9 %multiply_reduce_fusion = f32[128,2048]{1,0:T(8,128)S(1)} fusion(f32[128,2,2048]{2,1,0:T(2,128)} %reshape.176, f32[128,2]{1,0:T(8,128)S(1)} %copy.67), kind=kLoop, calls=%fused_computation.14 | loop fusion | flops 786432 | bytes 3146752 | tf_op jit(solution)/shard_map/reduce_sum | solution.py:139
  213.3 0.9 add_convert_fusion
  (64 shorter events, 0.3 us)
Async XLA Ops:
  7.2 135.7 %copy-start = (bf16[1,512,2048]{2,1,0:T(8,128)(2,1)S(1)}, bf16[1,512,2048]{2,1,0:T(8,128)(2,1)}, u32[]{:S(2)}) copy-start(bf16[1,512,2048]{2,1,0:T(8,128)(2,1)} %param.40) | copy-start | bytes 6291460
  7.2 54.0 %all-gather.2.cloned.1.call-start = ((), (), s32[]{:S(2)}) async-start(), calls=%async_computation.2 | async-start | bytes 4456448 | tf_op jit(solution)/shard_map/all_gather | solution.py:98
  19.0 3.1 %copy-start.6 = (bf16[128,2048]{1,0:T(8,128)(2,1)S(1)}, bf16[128,2048]{1,0:T(8,128)(2,1)}, u32[]{:S(2)}) copy-start(bf16[128,2048]{1,0:T(8,128)(2,1)} %param.21) | copy-start | bytes 1572868
  19.0 3.3 %copy-start.19 = (f32[64,64]{1,0:T(8,128)S(1)}, f32[64,64]{1,0:T(8,128)}, u32[]{:S(2)}) copy-start(f32[64,64]{1,0:T(8,128)} %param.26) | copy-start | bytes 49156
  19.1 3.3 %copy-start.20 = (f32[64,64]{1,0:T(8,128)S(1)}, f32[64,64]{1,0:T(8,128)}, u32[]{:S(2)}) copy-start(f32[64,64]{1,0:T(8,128)} %param.25) | copy-start | bytes 49156
  19.1 42.2 %copy-start.22 = (f32[2048]{0:T(1024)S(1)}, f32[2048]{0:T(1024)}, u32[]{:S(2)}) copy-start(f32[2048]{0:T(1024)} %param.23) | copy-start | bytes 24580
  23.2 43.5 %copy-start.8 = (f32[64,64,16]{1,2,0:T(8,128)S(1)}, f32[64,64,16]{1,2,0:T(8,128)}, u32[]{:S(2)}) copy-start(f32[64,64,16]{1,2,0:T(8,128)} %param.29) | copy-start | bytes 786436
  66.8 5.0 %copy-start.3 = (f32[1,128,4096]{1,2,0:T(8,128)S(1)}, f32[1,128,4096]{1,2,0:T(8,128)}, u32[]{:S(2)}) copy-start(f32[1,128,4096]{1,2,0:T(8,128)} %copy.58) | copy-start | bytes 6291460
  66.8 5.0 %copy-start.4 = (f32[1,128,4096]{1,2,0:T(8,128)S(1)}, f32[1,128,4096]{1,2,0:T(8,128)}, u32[]{:S(2)}) copy-start(f32[1,128,4096]{1,2,0:T(8,128)} %copy.59) | copy-start | bytes 6291460
  66.8 5.0 %copy-start.9 = (f32[64,64,16]{1,2,0:T(8,128)S(1)}, f32[64,64,16]{1,2,0:T(8,128)}, u32[]{:S(2)}) copy-start(f32[64,64,16]{1,2,0:T(8,128)} %param.28) | copy-start | bytes 786436
  66.8 4.9 %copy-start.13 = (f32[64,64]{1,0:T(8,128)S(1)}, f32[64,64]{1,0:T(8,128)}, u32[]{:S(2)}) copy-start(f32[64,64]{1,0:T(8,128)} %get-tuple-element.6) | copy-start | bytes 49156
  66.8 4.9 %copy-start.14 = (f32[64,64]{1,0:T(8,128)S(1)}, f32[64,64]{1,0:T(8,128)}, u32[]{:S(2)}) copy-start(f32[64,64]{1,0:T(8,128)} %get-tuple-element.7) | copy-start | bytes 49156
  66.8 4.9 %copy-start.15 = (f32[64,64]{1,0:T(8,128)S(1)}, f32[64,64]{1,0:T(8,128)}, u32[]{:S(2)}) copy-start(f32[64,64]{1,0:T(8,128)} %get-tuple-element.8) | copy-start | bytes 49156
  66.8 4.9 %copy-start.16 = (f32[64,64]{1,0:T(8,128)S(1)}, f32[64,64]{1,0:T(8,128)}, u32[]{:S(2)}) copy-start(f32[64,64]{1,0:T(8,128)} %get-tuple-element.9) | copy-start | bytes 49156
  71.8 5.2 %copy-start.2 = (f32[128,64,64]{0,2,1:T(8,128)}, f32[128,64,64]{0,2,1:T(8,128)S(1)}, u32[]{:S(2)}) copy-start(f32[128,64,64]{0,2,1:T(8,128)S(1)} %bitcast_add_fusion) | copy-start | bytes 6291460
  71.8 3.3 %copy-start.12 = (f32[64,16,64]{2,1,0:T(8,128)S(1)}, f32[64,16,64]{2,1,0:T(8,128)}, u32[]{:S(2)}) copy-start(f32[64,16,64]{2,1,0:T(8,128)} %param.30) | copy-start | bytes 786436
  75.0 3.9 %copy-start.1 = (f32[128,64,64]{0,2,1:T(8,128)}, f32[128,64,64]{0,2,1:T(8,128)S(1)}, u32[]{:S(2)}) copy-start(f32[128,64,64]{0,2,1:T(8,128)S(1)} %bitcast_add_fusion.1) | copy-start | bytes 6291460
  75.1 1.9 copy-start.11
  77.0 2.9 %copy-start.10 = (bf16[128,1024]{1,0:T(8,128)(2,1)S(1)}, bf16[128,1024]{1,0:T(8,128)(2,1)}, u32[]{:S(2)}) copy-start(bf16[128,1024]{1,0:T(8,128)(2,1)} %convolution_convert_fusion.2) | copy-start | bytes 786436
  77.0 2.9 %copy-start.26 = (f32[1024]{0:T(1024)S(1)}, f32[1024]{0:T(1024)}, u32[]{:S(2)}) copy-start(f32[1024]{0:T(1024)} %param.32) | copy-start | bytes 12292
  79.9 5.6 %copy-start.23 = (f32[2048]{0:T(1024)S(1)}, f32[2048]{0:T(1024)}, u32[]{:S(2)}) copy-start(f32[2048]{0:T(1024)} %param.35) | copy-start | bytes 24580
  87.7 52.9 %copy-start.25 = (bf16[1,2048,512]{2,1,0:T(8,128)(2,1)S(1)}, bf16[1,2048,512]{2,1,0:T(8,128)(2,1)}, u32[]{:S(2)}) copy-start(bf16[1,2048,512]{2,1,0:T(8,128)(2,1)} %param.38) | copy-start | bytes 6291460
  139.3 1.3 copy-start.7
  149.1 5.2 %copy-start.17 = (s32[128,2]{1,0:T(8,128)S(1)}, s32[128,2]{1,0:T(8,128)}, u32[]{:S(2)}) copy-start(s32[128,2]{1,0:T(8,128)} %get-tuple-element.10) | copy-start | bytes 3076
  149.1 5.4 %copy-start.24 = (s32[128,2]{0,1:T(2,128)S(1)}, s32[128,2]{0,1:T(2,128)}, u32[]{:S(2)}) copy-start(s32[128,2]{0,1:T(2,128)} %param.41) | copy-start | bytes 3076
  149.1 5.4 %copy-start.21 = (bf16[2048,4]{0,1:T(4,128)(2,1)S(1)}, bf16[2048,4]{0,1:T(4,128)(2,1)}, u32[]{:S(2)}) copy-start(bf16[2048,4]{0,1:T(4,128)(2,1)} %param.36) | copy-start | bytes 49156
  149.1 5.7 %copy-start.18 = (bf16[2048,16]{0,1:T(8,128)(2,1)S(1)}, bf16[2048,16]{0,1:T(8,128)(2,1)}, u32[]{:S(2)}) copy-start(bf16[2048,16]{0,1:T(8,128)(2,1)} %param.37) | copy-start | bytes 196612
  149.1 52.7 %all-to-all-start.1 = ((bf16[16,32,2048]{2,1,0:T(8,128)(2,1)}), bf16[16,32,2048]{2,1,0:T(8,128)(2,1)}, u32[]{:S(2)}, u32[]{:S(2)}) async-start(bf16[16,32,2048]{2,1,0:T(8,128)(2,1)} %bitcast.81), calls=%async_computation.1 | async-start | bytes 4194304 | tf_op jit(solution)/shard_map/all_to_all | solution.py:135
  208.4 4.9 %copy-start.5 = (f32[128,2048]{1,0:T(8,128)S(1)}, f32[128,2048]{1,0:T(8,128)}, u32[]{:S(2)}) copy-start(f32[128,2048]{1,0:T(8,128)} %get-tuple-element.13) | copy-start | bytes 3145732
Sparse Core Ops, SparseCore 0:
  10.1 51.0 all-gather.1
where the time goes:
time: 222 us; the launch traced here: 221 us
  waiting for transfers between devices  74.7 us (34%)
  blocking collectives  51.6 us (23%)
  matrix products  31.7 us (14%)
  local copies, waits for them, and re-layouts  28.9 us (13%)
  other arithmetic  14.5 us (7%)
  between operations  14.5 us (7%)
  starting transfers between devices  5.21 us (2%)
    all_to_all x1, blocking collectives, on_device(): lax.all_to_all(outgoing, 'ep', split_axis=0, concat_axis=0, tiled=True)  51.6 us
    all_gather x1, waiting for transfers between devices, on_device(): lax.all_gather(w_in, 'ep', axis=1, tiled=True)  38 us
    all_to_all x1, waiting for transfers between devices, on_device(): lax.all_to_all(result, 'ep', split_axis=0, concat_axis=0, tiled=True)  36.1 us
    slice x2, local copies, waits for them, and re-layouts, mixer_step(): old_re = state[0].reshape(rows, groups, entries)  7.65 us
    dot_general x1, matrix products, on_device(): jnp.einsum('erf,efd->erd', inner, w_down, preferred_element_type=jnp.floa...  6.23 us
    another operation x2, local copies, waits for them, and re-layouts, mixer_step(): new_state = jnp.stack([new_re.reshape(rows, -1), new_im.reshape(rows, -1)])  5.82 us
    dot_general x1, matrix products, on_device(): jnp.dot(glu, w_out, preferred_element_type=jnp.float32)  5.62 us
    all_to_all x1, starting transfers between devices, on_device(): lax.all_to_all(result, 'ep', split_axis=0, concat_axis=0, tiled=True)  5.17 us
  transfers between devices with their start and end apart: 2, of which 2 were waited for; matrix products, arithmetic and copies ran while one was open for 12% of the time, Pallas kernels for 0%

commit v1 on v0

v1 whole, which is shorter than its diff:
```python
import functools

import jax
import jax.numpy as jnp
from jax import lax
from jax.experimental import pallas as pl
from jax.experimental.pallas import tpu as pltpu
from jax.sharding import PartitionSpec as P

EXP_GROUPS = 4
TOPK = 2
QUAD = 4


def normalize(rows, gain):
    wide = rows.astype(jnp.float32)
    return wide * lax.rsqrt(jnp.mean(wide * wide, axis=-1, keepdims=True) + 1e-06) * gain


def discretize(lam_re, lam_im, log_step, in_re, in_im):
    step = jnp.exp(log_step)[:, None]
    magnitude = jnp.exp(lam_re * step)
    bar_re = magnitude * jnp.cos(lam_im * step)
    bar_im = magnitude * jnp.sin(lam_im * step)
    denom = lam_re * lam_re + lam_im * lam_im
    lessened = bar_re - 1.0
    coef_re = ((lessened * lam_re + bar_im * lam_im) / denom)[:, None, :]
    coef_im = ((bar_im * lam_re - lessened * lam_im) / denom)[:, None, :]
    in_re = in_re.transpose(0, 2, 1)
    in_im = in_im.transpose(0, 2, 1)
    drive_re = coef_re * in_re - coef_im * in_im
    drive_im = coef_re * in_im + coef_im * in_re
    return (bar_re, bar_im, drive_re, drive_im)


def split(wide):
    high = wide.astype(jnp.bfloat16)
    return high, (wide - high.astype(jnp.float32)).astype(jnp.bfloat16)


def dot(a, b):
    return jnp.dot(a, b, preferred_element_type=jnp.float32)


def dot_t(a, b):
    return lax.dot_general(a, b, (((1,), (1,)), ((), ())), preferred_element_type=jnp.float32)


def mixer_kernel(
    u_ref,
    state_ref,
    bar_ref,
    dre_ref,
    dim_ref,
    ore_ref,
    oim_ref,
    skip_ref,
    hidden_ref,
    gain_ref,
    router_ref,
    dispatch_ref,
    w_glu_ref,
    w_out_ref,
    new_ref,
    resid_ref,
    outgoing_ref,
    logits_ref,
    active_ref,
    glu_v,
    out_v,
    sems,
    *,
    width,
    entries,
):
    at = pl.program_id(0)
    last = pl.num_programs(0) - 1
    copy_glu = pltpu.make_async_copy(w_glu_ref, glu_v, sems.at[0])
    copy_out = pltpu.make_async_copy(w_out_ref, out_v, sems.at[1])

    @pl.when(at == 0)
    def _():
        copy_glu.start()
        copy_out.start()

    chans = u_ref.shape[1]
    lanes = state_ref.shape[2]
    row_group = lax.broadcasted_iota(jnp.int32, (chans, lanes), 0) // width
    lane_group = lax.broadcasted_iota(jnp.int32, (chans, lanes), 1) // entries
    same = row_group == lane_group

    def spread(ref):
        piece = ref[...]
        return jnp.where(same, jnp.concatenate([piece] * (lanes // piece.shape[1]), axis=1), 0.0)

    u = u_ref[...]
    drive_hi, drive_lo = split(jnp.concatenate([spread(dre_ref), spread(dim_ref)], axis=1))
    push = dot(jnp.concatenate([u, u], axis=1), jnp.concatenate([drive_hi, drive_lo], axis=0))
    bar_re = bar_ref[0:1, :]
    bar_im = bar_ref[1:2, :]
    old_re = state_ref[0]
    old_im = state_ref[1]
    new_re = bar_re * old_re - bar_im * old_im + push[:, :lanes]
    new_im = bar_re * old_im + bar_im * old_re + push[:, lanes:]
    new_ref[0] = new_re
    new_ref[1] = new_im
    new_hi, new_lo = split(jnp.concatenate([new_re, new_im], axis=1))
    read_hi, read_lo = split(jnp.concatenate([spread(ore_ref), -spread(oim_ref)], axis=1))
    read = dot_t(new_hi, read_hi) + dot_t(new_lo, read_hi) + dot_t(new_hi, read_lo)
    mixed = read + skip_ref[...] * u.astype(jnp.float32)
    active_ref[:, pl.ds(pl.multiple_of(at * chans, chans), chans)] = jax.nn.gelu(mixed)

    @pl.when(at == last)
    def _():
        copy_glu.wait()
        active = active_ref[...]
        gating = dot(active.astype(jnp.bfloat16), glu_v[...])
        glu = (active * jax.nn.sigmoid(gating)).astype(jnp.bfloat16)
        copy_out.wait()
        resid = (hidden_ref[...].astype(jnp.float32) + dot(glu, out_v[...])).astype(jnp.bfloat16)
        resid_ref[...] = resid
        normed = normalize(resid, gain_ref[...]).astype(jnp.bfloat16)
        outgoing_ref[...] = dot(dispatch_ref[...], normed).astype(jnp.bfloat16)
        logits_ref[...] = dot(normed, router_ref[...])


def mixer(u, state, bar, dre, dim, ore, oim, skip, hidden, gain, router, dispatch, w_glu, w_out, width, entries):
    rows, channels = u.shape
    chans = min(128, channels)
    steps = channels // chans
    lanes = chans // width * entries
    model = hidden.shape[1]

    def whole(a):
        return pl.BlockSpec(a.shape, lambda i: (0,) * a.ndim)

    along = pl.BlockSpec((chans, dre.shape[1]), lambda i: (i, 0))
    states = pl.BlockSpec((2, rows, lanes), lambda i: (0, 0, i))
    out_shape = (
        jax.ShapeDtypeStruct(state.shape, jnp.float32),
        jax.ShapeDtypeStruct(hidden.shape, jnp.bfloat16),
        jax.ShapeDtypeStruct((dispatch.shape[0], model), jnp.bfloat16),
        jax.ShapeDtypeStruct((rows, router.shape[1]), jnp.float32),
    )
    return pl.pallas_call(
        functools.partial(mixer_kernel, width=width, entries=entries),
        grid=(steps,),
        in_specs=[
            pl.BlockSpec((rows, chans), lambda i: (0, i)),
            states,
            pl.BlockSpec((2, lanes), lambda i: (0, i)),
            along,
            along,
            along,
            along,
            pl.BlockSpec((1, chans), lambda i: (0, i)),
            whole(hidden),
            whole(gain),
            whole(router),
            whole(dispatch),
            pl.BlockSpec(memory_space=pl.ANY),
            pl.BlockSpec(memory_space=pl.ANY),
        ],
        out_specs=(states,) + tuple(whole(s) for s in out_shape[1:]),
        out_shape=out_shape,
        scratch_shapes=[
            pltpu.VMEM((rows, channels), jnp.float32),
            pltpu.VMEM(w_glu.shape, w_glu.dtype),
            pltpu.VMEM(w_out.shape, w_out.dtype),
            pltpu.SemaphoreType.DMA((2,)),
        ],
        name="mixer",
    )(u, state, bar, dre, dim, ore, oim, skip, hidden, gain, router, dispatch, w_glu, w_out)


def combine_kernel(slot_ref, gates_ref, resid_ref, returned_ref, out_ref):
    slots = returned_ref.shape[0]
    rows = resid_ref.shape[0]
    lane = lax.broadcasted_iota(jnp.int32, (rows, slots), 1)
    weight = jnp.zeros((rows, slots), jnp.float32)
    for k in range(TOPK):
        weight = weight + jnp.where(slot_ref[:, k : k + 1] == lane, gates_ref[:, k : k + 1], 0.0)
    high, low = split(weight)
    returned = returned_ref[...]
    moe = dot(high, returned) + dot(low, returned)
    out_ref[...] = (resid_ref[...].astype(jnp.float32) + moe).astype(jnp.bfloat16)


def combine(slot, gates, resid, returned):
    model = resid.shape[1]
    piece = min(512, model)

    def column(a):
        return pl.BlockSpec((a.shape[0], piece), lambda i: (0, i))

    def whole(a):
        return pl.BlockSpec(a.shape, lambda i: (0, 0))

    return pl.pallas_call(
        combine_kernel,
        grid=(model // piece,),
        in_specs=[whole(slot), whole(gates), column(resid), column(returned)],
        out_specs=column(resid),
        out_shape=jax.ShapeDtypeStruct(resid.shape, jnp.bfloat16),
        name="combine",
    )(slot, gates, resid, returned)


def route_gates(group_logit, route_logit, route_ids, per_group):
    chosen = route_ids[:, 0] // per_group
    pick_group = (
        chosen[:, None] == jnp.arange(group_logit.shape[1], dtype=jnp.int32)[None, :]
    ).astype(jnp.float32)
    own = jnp.sum(group_logit * pick_group, axis=1, keepdims=True)
    group_weight = 1.0 / jnp.sum(jnp.exp(group_logit - own), axis=1)
    pick = (
        route_ids[:, :, None] == jnp.arange(route_logit.shape[1], dtype=jnp.int32)[None, None, :]
    ).astype(jnp.float32)
    chosen_logit = jnp.sum(pick * route_logit[:, None, :], axis=2)
    first = jax.nn.sigmoid(chosen_logit[:, 0] - chosen_logit[:, 1])
    pair = jnp.stack([first, 1.0 - first], axis=1)
    return group_weight[:, None] * pair


def project(normed, w_in):
    ranks = lax.axis_size("ep")
    me = lax.axis_index("ep")
    quads = ranks // QUAD
    rows = normed.shape[0]
    shard = w_in.shape[1]

    def across(a, k):
        return lax.ppermute(a, "ep", [(r, r ^ k) for r in range(ranks)])

    own = w_in.T
    shards = [own] + [
        lax.ppermute(own, "ep", [(r, (r + QUAD * d) % ranks) for r in range(ranks)])
        for d in range(1, quads)
    ]
    far = across(normed, 2)
    near = across(jnp.concatenate([normed, far], axis=0), 1)
    tokens = jnp.concatenate([normed, far, near], axis=0)
    table = jnp.concatenate(shards, axis=0)
    partial = dot_t(tokens, table).astype(jnp.bfloat16)
    order = (0, 2, 1, 3)
    pieces = [partial[:rows]] + [
        across(partial[i * rows : (i + 1) * rows], order[i]) for i in range(1, QUAD)
    ]
    joined = jnp.concatenate(pieces, axis=1)
    total = ranks * shard
    source = jnp.arange(total, dtype=jnp.int32)
    which, offset, inside = source // (quads * shard), source // shard % quads, source % shard
    k = jnp.where(which == 1, 2, jnp.where(which == 2, 1, which))
    rank = (me // QUAD - offset) % quads * QUAD + ((me % QUAD) ^ k)
    target = rank * shard + inside
    turn = (target[:, None] == jnp.arange(total, dtype=jnp.int32)[None, :]).astype(jnp.bfloat16)
    return dot(joined, turn).astype(jnp.bfloat16)


def on_device(
    hidden,
    state,
    norm_gain,
    w_in,
    lam_re,
    lam_im,
    log_step,
    in_re,
    in_im,
    out_re,
    out_im,
    skip,
    w_glu,
    w_out,
    ffn_gain,
    w_group,
    w_route,
    w_gate,
    w_up,
    w_down,
    route_ids,
):
    groups, entries = lam_re.shape
    width = in_re.shape[2]
    count_dev, model_width = hidden.shape
    experts = w_route.shape[1]
    sources = lax.axis_size("ep")
    normed = normalize(hidden, norm_gain).astype(jnp.bfloat16)
    inputs = project(normed, w_in)

    bar_re, bar_im, drive_re, drive_im = discretize(lam_re, lam_im, log_step, in_re, in_im)
    bar = jnp.stack([bar_re.reshape(-1), bar_im.reshape(-1)])
    copies = max(1, 128 // entries)

    def lined(a):
        return jnp.tile(a.reshape(groups * width, entries), (1, copies))

    capacity = 2 * TOPK * count_dev // experts
    flat = route_ids.reshape(-1)
    hits = (flat[:, None] == jnp.arange(experts, dtype=jnp.int32)[None, :]).astype(jnp.int32)
    before = jnp.sum((jnp.cumsum(hits, axis=0) - hits) * hits, axis=1)
    slot = (flat * capacity + before).reshape(count_dev, TOPK)
    lane = jnp.arange(experts * capacity, dtype=jnp.int32)
    dispatch = jnp.any(slot.T[:, None, :] == lane[None, :, None], axis=0).astype(jnp.bfloat16)
    router = jnp.concatenate([w_group, w_route], axis=1)
    used = router.shape[1]
    router = jnp.pad(router, ((0, 0), (0, -used % 128)))

    new_state, resid, outgoing, logits = mixer(
        inputs,
        state,
        bar,
        lined(drive_re),
        lined(drive_im),
        lined(out_re),
        lined(out_im),
        skip[None, :],
        hidden,
        ffn_gain[None, :],
        router,
        dispatch,
        w_glu,
        w_out,
        width,
        entries,
    )
    received = lax.all_to_all(
        outgoing.reshape(experts, capacity, model_width), "ep", split_axis=0, concat_axis=0, tiled=True
    )
    arranged = received.reshape(experts * capacity, model_width)
    gate = dot(arranged, w_gate[0])
    upper = dot(arranged, w_up[0])
    inner = (jax.nn.silu(gate) * upper).astype(jnp.bfloat16)
    result = dot(inner, w_down[0]).astype(jnp.bfloat16)
    returned = lax.all_to_all(
        result.reshape(sources, capacity, model_width), "ep", split_axis=0, concat_axis=0, tiled=True
    )
    groups_used = w_group.shape[1]
    gates = route_gates(
        logits[:, :groups_used], logits[:, groups_used:used], route_ids, experts // EXP_GROUPS
    )
    hidden_out = combine(slot, gates, resid, returned.reshape(experts * capacity, model_width))
    return (hidden_out, new_state)


def solution(mesh):
    return jax.shard_map(
        on_device,
        mesh=mesh,
        in_specs=(
            P(("grp", "ep"), None),
            P(None, ("grp", "ep"), None),
            P(),
            P(None, "ep"),
            P(),
            P(),
            P(),
            P(),
            P(),
            P(),
            P(),
            P(),
            P(),
            P(),
            P(),
            P(),
            P(),
            P("ep", None, None),
            P("ep", None, None),
            P("ep", None, None),
            P(("grp", "ep"), None),
        ),
        out_specs=(P(("grp", "ep"), None), P(None, ("grp", "ep"), None)),
        check_vma=False,
    )
```

time: 222 us -> 181 us (0.82)
  matrix products: 31.7 us -> 11.4 us
  Pallas kernels: 0 us -> 18.7 us
  waiting for transfers between devices: 74.7 us -> 56.8 us
  local copies, waits for them, and re-layouts: 28.9 us -> 13.5 us
  between operations: 14.5 us -> 0.98 us
  starting transfers between devices: 5.21 us -> 14.5 us
  other arithmetic: 14.5 us -> 11.8 us
    all_gather x1 -> x0, waiting for transfers between devices: 38 us -> none  [on_device(): lax.all_gather(w_in, 'ep', axis=1, tiled=True)]
    dot_general x11 -> x4, matrix products: 31.7 us -> 11.4 us  [the longest x3 8.9 us: dot(): return jnp.dot(a, b, preferred_element_type=jnp.float32)]
    pallas_call x0 -> x2, Pallas kernels: none -> 18.7 us  [the longest x1 14.3 us: mixer(): pl.pallas_call(functools.partial(mixer_kernel, width=width, entries=entri...]
    ppermute x0 -> x8, waiting for transfers between devices: none -> 10.8 us  [the longest x5 10.8 us: across(): return lax.ppermute(a, 'ep', [(r, r ^ k) for r in range(ranks)])]
    slice x4, local copies, waits for them, and re-layouts: 10.8 us -> 0.36 us  [the longest x2 7.65 us: mixer_step(): old_re = state[0].reshape(rows, groups, entries)]
    all_to_all x1, waiting for transfers between devices: 36.1 us -> 46.1 us  [on_device(): lax.all_to_all(result.reshape(sources, capacity, model_width), 'ep', spli...]
    ppermute x0 -> x8, starting transfers between devices: none -> 9.32 us  [the longest x3 4.73 us: project(): lax.ppermute(own, 'ep', [(r, (r + QUAD * d) % ranks) for r in range(ranks)])]
    reduce_sum x2 -> x1, other arithmetic: 5 us -> 0.18 us  [route_gates(): own = jnp.sum(group_logit * pick_group, axis=1, keepdims=True)]
  transfers between devices with their start and end apart: 2 -> 9, of which waited for: 2 -> 4; matrix products, arithmetic and copies ran while one was open for 12% -> 13% of each run, Pallas kernels for 0% -> 0%
where the time goes in v1:
time: 181 us
  waiting for transfers between devices  56.8 us (31%)
  blocking collectives  52.9 us (29%)
  Pallas kernels  18.7 us (10%)
  starting transfers between devices  14.5 us (8%)
  local copies, waits for them, and re-layouts  13.5 us (7%)
  other arithmetic  11.8 us (7%)
  matrix products  11.4 us (6%)
    all_to_all x1, blocking collectives, on_device(): lax.all_to_all(outgoing.reshape(experts, capacity, model_width), 'ep', sp...  52.9 us
    all_to_all x1, waiting for transfers between devices, on_device(): lax.all_to_all(result.reshape(sources, capacity, model_width), 'ep', spli...  46.1 us
    pallas_call x1, Pallas kernels, mixer(): pl.pallas_call(functools.partial(mixer_kernel, width=width, entries=entri...  14.3 us
    ppermute x5, waiting for transfers between devices, across(): return lax.ppermute(a, 'ep', [(r, r ^ k) for r in range(ranks)])  10.8 us
    dot_general x3, matrix products, dot(): return jnp.dot(a, b, preferred_element_type=jnp.float32)  8.9 us
    another operation x12, local copies, waits for them, and re-layouts, lined(): return jnp.tile(a.reshape(groups * width, entries), (1, copies))  7.57 us
    all_to_all x1, starting transfers between devices, on_device(): lax.all_to_all(result.reshape(sources, capacity, model_width), 'ep', spli...  5.15 us
    ppermute x3, starting transfers between devices, project(): lax.ppermute(own, 'ep', [(r, (r + QUAD * d) % ranks) for r in range(ranks)])  4.73 us
  transfers between devices with their start and end apart: 9, of which 4 were waited for; matrix products, arithmetic and copies ran while one was open for 13% of the time, Pallas kernels for 0%

profile of v1, /device:TPU:13, one launch (start us, length us, event | category | flops | bytes accessed | tf_op | source)
XLA Modules:
  0.0 180.5 jit_solution(13105387959668003801)
XLA Ops:
  0.7 0.2 collective-permute-start.4
  0.9 2.3 %collective-permute-start.3 = (bf16[64,2048]{1,0:T(8,128)(2,1)}, bf16[64,2048]{1,0:T(8,128)(2,1)}, u32[]{:S(2)}, u32[]{:S(2)}) collective-permute-start(bf16[64,2048]{1,0:T(8,128)(2,1)} %bitcast.74), channel_id=1, source_target_pairs={{0,8},{1,9},{2,10},{3,11},{4,12},{5,13},{6,14},{7,15},{8,0},{9,1},... | collective-permute-start | bytes 786440 | tf_op jit(solution)/shard_map/ppermute | solution.py:237
  3.2 2.2 %collective-permute-start.2 = (bf16[64,2048]{1,0:T(8,128)(2,1)}, bf16[64,2048]{1,0:T(8,128)(2,1)}, u32[]{:S(2)}, u32[]{:S(2)}) collective-permute-start(bf16[64,2048]{1,0:T(8,128)(2,1)} %bitcast.75), channel_id=1, source_target_pairs={{0,4},{1,5},{2,6},{3,7},{4,8},{5,9},{6,10},{7,11},{8,12},{9,13},{1... | collective-permute-start | bytes 786440 | tf_op jit(solution)/shard_map/ppermute | solution.py:237
  5.4 1.2 fusion.23
  6.6 1.3 fusion.25
  7.9 0.3 collective-permute-start
  8.2 0.8 copy.80
  9.2 0.7 broadcast_multiply_fusion.1
  10.0 0.7 exp.18
  10.8 0.6 reduce-window.6
  11.4 0.2 slice_reduce_fusion
  11.9 0.2 fusion.44
  12.2 7.9 %collective-permute-done = bf16[128,2048]{1,0:T(8,128)(2,1)} collective-permute-done((bf16[128,2048]{1,0:T(8,128)(2,1)S(1)}, bf16[128,2048]{1,0:T(8,128)(2,1)}, u32[]{:S(2)}, u32[]{:S(2)}) %collective-permute-start) | collective-permute-done | bytes 524320 | tf_op jit(solution)/shard_map/ppermute | solution.py:233
  20.1 2.1 %pad_maximum_fusion = bf16[256,2048]{1,0:T(8,128)(2,1)} fusion(bf16[128,2048]{1,0:T(8,128)(2,1)} %collective-permute-done, bf16[128,2048]{1,0:T(8,128)(2,1)S(1)} %fusion.25), kind=kLoop, calls=%fused_computation.24 | loop fusion | flops 2097152 | bytes 2097152 | tf_op jit(solution)/shard_map/concatenate | solution.py:241
  22.2 2.4 %collective-permute-start.1 = (bf16[256,2048]{1,0:T(8,128)(2,1)}, bf16[256,2048]{1,0:T(8,128)(2,1)}, u32[]{:S(2)}, u32[]{:S(2)}) collective-permute-start(bf16[256,2048]{1,0:T(8,128)(2,1)} %pad_maximum_fusion), channel_id=1, source_target_pairs={{0,1},{1,0},{2,3},{3,2},{4,5},{5,4},{6,7},{7,6},{8,9},{9,8},{10,11... | collective-permute-start | bytes 3145736 | tf_op jit(solution)/shard_map/ppermute | solution.py:233
  24.6 0.7 convert_element_type.39.dispatch_ref
  25.4 0.7 stack_reshape.6
  26.1 0.2 copy.86
  26.4 1.0 copy.92.ore_ref
  27.4 0.2 copy.87
  27.6 1.0 copy.93.oim_ref
  28.6 0.7 pad_maximum_fusion.1
  29.4 0.3 copy.88
  29.7 2.2 %multiply_add_fusion = (f32[64,64,16]{1,2,0:T(8,128)}, f32[64,64,16]{1,2,0:T(8,128)S(1)}) fusion(f32[64,64,16]{1,2,0:T(8,128)} %param.28, f32[64,64,16]{1,2,0:T(8,128)} %param.29, f32[64,64]{1,0:T(8,128)S(1)} %get-tuple-element.21, f32[64,64]{1,0:T(8,128)S(1)} %get-tuple-element.18), kind=kLoop, calls=%fused_computation.34 | loop fusion | flops 393216 | bytes 1081344 | tf_op jit(solution)/shard_map/add | solution.py:32
  31.8 1.2 copy.85
  33.1 0.9 copy.84
  33.9 1.0 tile.41
  35.0 1.0 copy.90.dre_ref
  36.0 1.0 copy.91.dim_ref
  37.0 0.9 pad.4.router_ref
  37.9 0.6 pad_maximum_fusion.2.bar_ref
  38.6 2.5 %fusion.19 = bf16[512,256]{0,1:T(8,128)(2,1)S(1)} fusion(bf16[256,2048]{1,0:T(8,128)(2,1)} %collective-permute-done.1, bf16[128,2048]{1,0:T(8,128)(2,1)} %collective-permute-done, bf16[128,2048]{1,0:T(8,128)(2,1)} %copy-done.2, bf16[64,2048]{1,0:T(8,128)(2,1)} %collective-permute-done.4, bf16[64,2048]{1,0:T(8,128)(2,1)} %collective-permute-done.3, ...), kind=kOutput, calls=%fused_computation.19 | convolution fusion | flops 547487744 | bytes 3407872 | tf_op jit(solution)/shard_map/dot_general | solution.py:46
  41.3 0.5 collective-permute-start.6
  41.9 1.2 collective-permute-start.5
  43.1 2.5 %collective-permute-done.7 = bf16[128,256]{0,1:T(8,128)(2,1)S(1)} collective-permute-done((bf16[128,256]{0,1:T(8,128)(2,1)S(1)}, bf16[128,256]{0,1:T(8,128)(2,1)S(1)}, u32[]{:S(2)}, u32[]{:S(2)}) %collective-permute-start.7) | collective-permute-done | bytes 65568 | tf_op jit(solution)/shard_map/ppermute | solution.py:233
  45.6 0.4 collective-permute-done.5
  46.0 1.7 fusion.22.u_ref
  47.6 14.3 %mixer.1 = (f32[2,128,4096]{2,1,0:T(8,128)}, bf16[128,2048]{1,0:T(8,128)(2,1)}, bf16[512,2048]{1,0:T(8,128)(2,1)}, f32[128,128]{1,0:T(8,128)}) custom-call(bf16[128,1024]{1,0:T(8,128)(2,1)} %fusion.22.u_ref, f32[2,128,4096]{2,1,0:T(8,128)} %state_ref.1, f32[2,4096]{1,0:T(2,128)} %pad_maximum_fusion.2.bar_ref, f32[1024,128]{1,0:T(8,128)} %copy.90.dre_ref, ...), custom_call_target="tpu_custom_call" | custom-call | tf_op jit(solution)/shard_map/mixer/pallas_call | solution.py:145
  61.9 52.9 %all_to_all.10 = bf16[16,32,2048]{2,1,0:T(8,128)(2,1)S(1)} all-to-all(bf16[16,32,2048]{2,1,0:T(8,128)(2,1)} %bitcast.59), channel_id=1, replica_groups=mesh['grp'=2,'ep'=16] {'ep'}, dimensions={0} | all-to-all | bytes 4194304 | tf_op jit(solution)/shard_map/all_to_all | solution.py:327
  114.9 1.3 copy-done.1
  116.2 1.2 fusion.10
  117.4 6.0 %convolution_convert_fusion = bf16[512,2048]{1,0:T(8,128)(2,1)} fusion(bf16[1,512,2048]{2,1,0:T(8,128)(2,1)S(1)} %copy-done, bf16[512,2048]{1,0:T(8,128)(2,1)} %bitcast.61, bf16[1,2048,512]{2,1,0:T(8,128)(2,1)} %param.39, f32[512,512]{1,0:T(8,128)S(1)} %fusion.10), kind=kOutput, calls=%fused_computation.2 | convolution fusion | flops 2150105088 | bytes 9437184 | tf_op jit(solution)/shard_map/dot_general | solution.py:42
  123.4 5.1 %all-to-all-start.1 = ((bf16[16,32,2048]{2,1,0:T(8,128)(2,1)}), bf16[16,32,2048]{2,1,0:T(8,128)(2,1)}, u32[]{:S(2)}, u32[]{:S(2)}) async-start(bf16[16,32,2048]{2,1,0:T(8,128)(2,1)} %bitcast.58), calls=%async_computation.1 | async-start | bytes 4194304 | tf_op jit(solution)/shard_map/all_to_all | solution.py:335
  128.9 0.2 select_reduce_fusion
  129.1 0.2 exponential_reduce_fusion
  129.3 0.7 broadcast_multiply_fusion.gates_ref
  130.0 46.1 %all-to-all-done.1 = bf16[16,32,2048]{2,1,0:T(8,128)(2,1)} async-done(((bf16[16,32,2048]{2,1,0:T(8,128)(2,1)}), bf16[16,32,2048]{2,1,0:T(8,128)(2,1)}, u32[]{:S(2)}, u32[]{:S(2)}) %all-to-all-start.1) | async-done | bytes 2097184 | tf_op jit(solution)/shard_map/all_to_all | solution.py:335
  176.1 4.4 %combine.1 = bf16[128,2048]{1,0:T(8,128)(2,1)} custom-call(s32[128,2]{1,0:T(8,128)} %copy-done.3, f32[128,2]{1,0:T(8,128)} %broadcast_multiply_fusion.gates_ref, bf16[128,2048]{1,0:T(8,128)(2,1)} %get-tuple-element.7.resid_ref, bf16[512,2048]{1,0:T(8,128)(2,1)} %bitcast.22.returned_ref), custom_call_target="tpu_custom_call" | custom-call | tf_op jit(solution)/shard_map/combine/pallas_call | solution.py:199
  (59 shorter events, 1.7 us)
Async XLA Ops:
  0.6 116.8 %copy-start = (bf16[1,512,2048]{2,1,0:T(8,128)(2,1)S(1)}, bf16[1,512,2048]{2,1,0:T(8,128)(2,1)}, u32[]{:S(2)}) copy-start(bf16[1,512,2048]{2,1,0:T(8,128)(2,1)} %param.40) | copy-start | bytes 6291460
  0.6 11.3 %copy-start.9 = (f32[64,64]{1,0:T(8,128)S(1)}, f32[64,64]{1,0:T(8,128)}, u32[]{:S(2)}) copy-start(f32[64,64]{1,0:T(8,128)} %param.26) | copy-start | bytes 49156
  0.7 11.3 %copy-start.10 = (f32[64,64]{1,0:T(8,128)S(1)}, f32[64,64]{1,0:T(8,128)}, u32[]{:S(2)}) copy-start(f32[64,64]{1,0:T(8,128)} %param.25) | copy-start | bytes 49156
  0.7 37.9 %collective-permute-start.4 = (bf16[64,2048]{1,0:T(8,128)(2,1)}, bf16[64,2048]{1,0:T(8,128)(2,1)}, u32[]{:S(2)}, u32[]{:S(2)}) collective-permute-start(bf16[64,2048]{1,0:T(8,128)(2,1)} %bitcast.73), channel_id=1, source_target_pairs={{0,12},{1,13},{2,14},{3,15},{4,0},{5,1},{6,2},{7,3},{8,4},{9,5},{1... | collective-permute-start | bytes 786440 | tf_op jit(solution)/shard_map/ppermute | solution.py:237
  0.9 37.7 %collective-permute-start.3 = (bf16[64,2048]{1,0:T(8,128)(2,1)}, bf16[64,2048]{1,0:T(8,128)(2,1)}, u32[]{:S(2)}, u32[]{:S(2)}) collective-permute-start(bf16[64,2048]{1,0:T(8,128)(2,1)} %bitcast.74), channel_id=1, source_target_pairs={{0,8},{1,9},{2,10},{3,11},{4,12},{5,13},{6,14},{7,15},{8,0},{9,1},... | collective-permute-start | bytes 786440 | tf_op jit(solution)/shard_map/ppermute | solution.py:237
  3.2 35.4 %collective-permute-start.2 = (bf16[64,2048]{1,0:T(8,128)(2,1)}, bf16[64,2048]{1,0:T(8,128)(2,1)}, u32[]{:S(2)}, u32[]{:S(2)}) collective-permute-start(bf16[64,2048]{1,0:T(8,128)(2,1)} %bitcast.75), channel_id=1, source_target_pairs={{0,4},{1,5},{2,6},{3,7},{4,8},{5,9},{6,10},{7,11},{8,12},{9,13},{1... | collective-permute-start | bytes 786440 | tf_op jit(solution)/shard_map/ppermute | solution.py:237
  6.6 19.5 %copy-start.5 = (f32[64,16,64]{2,1,0:T(8,128)S(1)}, f32[64,16,64]{2,1,0:T(8,128)}, u32[]{:S(2)}) copy-start(f32[64,16,64]{2,1,0:T(8,128)} %param.30) | copy-start | bytes 786436
  7.9 18.2 %copy-start.2 = (bf16[128,2048]{1,0:T(8,128)(2,1)}, bf16[128,2048]{1,0:T(8,128)(2,1)S(1)}, u32[]{:S(2)}) copy-start(bf16[128,2048]{1,0:T(8,128)(2,1)S(1)} %fusion.25) | copy-start | bytes 1572868
  7.9 12.1 %collective-permute-start = (bf16[128,2048]{1,0:T(8,128)(2,1)S(1)}, bf16[128,2048]{1,0:T(8,128)(2,1)}, u32[]{:S(2)}, u32[]{:S(2)}) collective-permute-start(bf16[128,2048]{1,0:T(8,128)(2,1)S(1)} %fusion.25), channel_id=1, source_target_pairs={{0,2},{1,3},{2,0},{3,1},{4,6},{5,7},{6,4},{7,5},{8,10},{9,11},{10,... | collective-permute-start | bytes 1572872 | tf_op jit(solution)/shard_map/ppermute | solution.py:233
  11.9 14.5 %copy-start.3 = (s32[128,2]{1,0:T(8,128)}, s32[128,2]{1,0:T(8,128)S(1)}, u32[]{:S(2)}) copy-start(s32[128,2]{1,0:T(8,128)S(1)} %add.96.slot_ref) | copy-start | bytes 3076
  22.2 16.4 %collective-permute-start.1 = (bf16[256,2048]{1,0:T(8,128)(2,1)}, bf16[256,2048]{1,0:T(8,128)(2,1)}, u32[]{:S(2)}, u32[]{:S(2)}) collective-permute-start(bf16[256,2048]{1,0:T(8,128)(2,1)} %pad_maximum_fusion), channel_id=1, source_target_pairs={{0,1},{1,0},{2,3},{3,2},{4,5},{5,4},{6,7},{7,6},{8,9},{9,8},{10,11... | collective-permute-start | bytes 3145736 | tf_op jit(solution)/shard_map/ppermute | solution.py:233
  26.3 1.1 copy-start.6
  26.4 2.2 %copy-start.8 = (bf16[2048,16]{0,1:T(8,128)(2,1)S(1)}, bf16[2048,16]{0,1:T(8,128)(2,1)}, u32[]{:S(2)}) copy-start(bf16[2048,16]{0,1:T(8,128)(2,1)} %param.37) | copy-start | bytes 196612
  34.9 3.0 %copy-start.7 = (f32[1,4096]{1,0:T(1,128)S(1)}, f32[1,4096]{1,0:T(1,128)}, u32[]{:S(2)}) copy-start(f32[1,4096]{1,0:T(1,128)} %stack_reshape.6) | copy-start | bytes 49156
  36.0 2.6 %copy-start.13 = (bf16[2048,64]{0,1:T(8,128)(2,1)S(1)}, bf16[2048,64]{0,1:T(8,128)(2,1)}, u32[]{:S(2)}) copy-start(bf16[2048,64]{0,1:T(8,128)(2,1)} %param.24) | copy-start | bytes 786436
  41.2 4.4 %collective-permute-start.7 = (bf16[128,256]{0,1:T(8,128)(2,1)S(1)}, bf16[128,256]{0,1:T(8,128)(2,1)S(1)}, u32[]{:S(2)}, u32[]{:S(2)}) collective-permute-start(bf16[128,256]{0,1:T(8,128)(2,1)S(1)} %get-tuple-element.15), channel_id=1, source_target_pairs={{0,3},{1,2},{2,1},{3,0},{4,7},{5,6},{6,5},{7,4},{8,11},{9,10},{10,... | collective-permute-start | bytes 196616 | tf_op jit(solution)/shard_map/ppermute | solution.py:233
  41.3 4.3 %collective-permute-start.6 = (bf16[128,256]{0,1:T(8,128)(2,1)S(1)}, bf16[128,256]{0,1:T(8,128)(2,1)S(1)}, u32[]{:S(2)}, u32[]{:S(2)}) collective-permute-start(bf16[128,256]{0,1:T(8,128)(2,1)S(1)} %get-tuple-element.16), channel_id=1, source_target_pairs={{0,1},{1,0},{2,3},{3,2},{4,5},{5,4},{6,7},{7,6},{8,9},{9,8},{10,11... | collective-permute-start | bytes 196616 | tf_op jit(solution)/shard_map/ppermute | solution.py:233
  41.9 4.1 %collective-permute-start.5 = (bf16[128,256]{0,1:T(8,128)(2,1)S(1)}, bf16[128,256]{0,1:T(8,128)(2,1)S(1)}, u32[]{:S(2)}, u32[]{:S(2)}) collective-permute-start(bf16[128,256]{0,1:T(8,128)(2,1)S(1)} %get-tuple-element.17), channel_id=1, source_target_pairs={{0,2},{1,3},{2,0},{3,1},{4,6},{5,7},{6,4},{7,5},{8,10},{9,11},{10,... | collective-permute-start | bytes 196616 | tf_op jit(solution)/shard_map/ppermute | solution.py:233
  61.9 54.3 %copy-start.12 = (bf16[1,2048,512]{2,1,0:T(8,128)(2,1)S(1)}, bf16[1,2048,512]{2,1,0:T(8,128)(2,1)}, u32[]{:S(2)}) copy-start(bf16[1,2048,512]{2,1,0:T(8,128)(2,1)} %param.38) | copy-start | bytes 6291460
  114.8 1.3 copy-start.1
  123.4 5.2 %copy-start.11 = (s32[128,2]{0,1:T(2,128)S(1)}, s32[128,2]{0,1:T(2,128)}, u32[]{:S(2)}) copy-start(s32[128,2]{0,1:T(2,128)} %param.41) | copy-start | bytes 3076
  123.4 5.2 %copy-start.4 = (f32[128,128]{1,0:T(8,128)S(1)}, f32[128,128]{1,0:T(8,128)}, u32[]{:S(2)}) copy-start(f32[128,128]{1,0:T(8,128)} %get-tuple-element.6) | copy-start | bytes 196612
  123.4 52.7 %all-to-all-start.1 = ((bf16[16,32,2048]{2,1,0:T(8,128)(2,1)}), bf16[16,32,2048]{2,1,0:T(8,128)(2,1)}, u32[]{:S(2)}, u32[]{:S(2)}) async-start(bf16[16,32,2048]{2,1,0:T(8,128)(2,1)} %bitcast.58), calls=%async_computation.1 | async-start | bytes 4194304 | tf_op jit(solution)/shard_map/all_to_all | solution.py:335

commit v2 on v1

--- a/solution.py
+++ b/solution.py
@@ -57,17 +57,17 @@
     skip_ref,
     hidden_ref,
     gain_ref,
-    router_ref,
     dispatch_ref,
     w_glu_ref,
     w_out_ref,
     new_ref,
     resid_ref,
     outgoing_ref,
-    logits_ref,
+    normed_ref,
     active_ref,
     glu_v,
     out_v,
+    same_ref,
     sems,
     *,
     width,
@@ -85,17 +85,23 @@
 
     chans = u_ref.shape[1]
     lanes = state_ref.shape[2]
-    row_group = lax.broadcasted_iota(jnp.int32, (chans, lanes), 0) // width
-    lane_group = lax.broadcasted_iota(jnp.int32, (chans, lanes), 1) // entries
-    same = row_group == lane_group
+
+    @pl.when(at == 0)
+    def _():
+        row_group = lax.broadcasted_iota(jnp.int32, (chans, lanes), 0) // width
+        lane_group = lax.broadcasted_iota(jnp.int32, (chans, lanes), 1) // entries
+        same_ref[...] = (row_group == lane_group).astype(jnp.float32).astype(jnp.bfloat16)
+
+    same = same_ref[...]
 
     def spread(ref):
         piece = ref[...]
-        return jnp.where(same, jnp.concatenate([piece] * (lanes // piece.shape[1]), axis=1), 0.0)
+        twice = split(jnp.concatenate([piece, piece], axis=1))
+        return [jnp.concatenate([h] * (lanes // h.shape[1]), axis=1) * same for h in twice]
 
     u = u_ref[...]
-    drive_hi, drive_lo = split(jnp.concatenate([spread(dre_ref), spread(dim_ref)], axis=1))
-    push = dot(jnp.concatenate([u, u], axis=1), jnp.concatenate([drive_hi, drive_lo], axis=0))
+    drive = [jnp.concatenate(pair, axis=1) for pair in zip(spread(dre_ref), spread(dim_ref))]
+    push = dot(jnp.concatenate([u, u], axis=1), jnp.concatenate(drive, axis=0))
     bar_re = bar_ref[0:1, :]
     bar_im = bar_ref[1:2, :]
     old_re = state_ref[0]
@@ -105,7 +111,9 @@
     new_ref[0] = new_re
     new_ref[1] = new_im
     new_hi, new_lo = split(jnp.concatenate([new_re, new_im], axis=1))
-    read_hi, read_lo = split(jnp.concatenate([spread(ore_ref), -spread(oim_ref)], axis=1))
+    read_hi, read_lo = [
+        jnp.concatenate([real, -imag], axis=1) for real, imag in zip(spread(ore_ref), spread(oim_ref))
+    ]
     read = dot_t(new_hi, read_hi) + dot_t(new_lo, read_hi) + dot_t(new_hi, read_lo)
     mixed = read + skip_ref[...] * u.astype(jnp.float32)
     active_ref[:, pl.ds(pl.multiple_of(at * chans, chans), chans)] = jax.nn.gelu(mixed)
@@ -121,10 +129,10 @@
         resid_ref[...] = resid
         normed = normalize(resid, gain_ref[...]).astype(jnp.bfloat16)
         outgoing_ref[...] = dot(dispatch_ref[...], normed).astype(jnp.bfloat16)
-        logits_ref[...] = dot(normed, router_ref[...])
-
-
-def mixer(u, state, bar, dre, dim, ore, oim, skip, hidden, gain, router, dispatch, w_glu, w_out, width, entries):
+        normed_ref[...] = normed
+
+
+def mixer(u, state, bar, dre, dim, ore, oim, skip, hidden, gain, dispatch, w_glu, w_out, width, entries):
     rows, channels = u.shape
     chans = min(128, channels)
     steps = channels // chans
@@ -140,7 +148,7 @@
         jax.ShapeDtypeStruct(state.shape, jnp.float32),
         jax.ShapeDtypeStruct(hidden.shape, jnp.bfloat16),
         jax.ShapeDtypeStruct((dispatch.shape[0], model), jnp.bfloat16),
-        jax.ShapeDtypeStruct((rows, router.shape[1]), jnp.float32),
+        jax.ShapeDtypeStruct(hidden.shape, jnp.bfloat16),
     )
     return pl.pallas_call(
         functools.partial(mixer_kernel, width=width, entries=entries),
@@ -156,7 +164,6 @@
             pl.BlockSpec((1, chans), lambda i: (0, i)),
             whole(hidden),
             whole(gain),
-            whole(router),
             whole(dispatch),
             pl.BlockSpec(memory_space=pl.ANY),
             pl.BlockSpec(memory_space=pl.ANY),
@@ -167,22 +174,27 @@
             pltpu.VMEM((rows, channels), jnp.float32),
             pltpu.VMEM(w_glu.shape, w_glu.dtype),
             pltpu.VMEM(w_out.shape, w_out.dtype),
+            pltpu.VMEM((chans, lanes), jnp.bfloat16),
             pltpu.SemaphoreType.DMA((2,)),
         ],
         name="mixer",
-    )(u, state, bar, dre, dim, ore, oim, skip, hidden, gain, router, dispatch, w_glu, w_out)
-
-
-def combine_kernel(slot_ref, gates_ref, resid_ref, returned_ref, out_ref):
+    )(u, state, bar, dre, dim, ore, oim, skip, hidden, gain, dispatch, w_glu, w_out)
+
+
+def combine_kernel(slot_ref, gates_ref, resid_ref, returned_ref, out_ref, high_ref, low_ref):
     slots = returned_ref.shape[0]
     rows = resid_ref.shape[0]
-    lane = lax.broadcasted_iota(jnp.int32, (rows, slots), 1)
-    weight = jnp.zeros((rows, slots), jnp.float32)
-    for k in range(TOPK):
-        weight = weight + jnp.where(slot_ref[:, k : k + 1] == lane, gates_ref[:, k : k + 1], 0.0)
-    high, low = split(weight)
+
+    @pl.when(pl.program_id(0) == 0)
+    def _():
+        lane = lax.broadcasted_iota(jnp.int32, (rows, slots), 1)
+        weight = jnp.zeros((rows, slots), jnp.float32)
+        for k in range(TOPK):
+            weight = weight + jnp.where(slot_ref[:, k : k + 1] == lane, gates_ref[:, k : k + 1], 0.0)
+        high_ref[...], low_ref[...] = split(weight)
+
     returned = returned_ref[...]
-    moe = dot(high, returned) + dot(low, returned)
+    moe = dot(high_ref[...], returned) + dot(low_ref[...], returned)
     out_ref[...] = (resid_ref[...].astype(jnp.float32) + moe).astype(jnp.bfloat16)
 
 
@@ -202,6 +214,7 @@
         in_specs=[whole(slot), whole(gates), column(resid), column(returned)],
         out_specs=column(resid),
         out_shape=jax.ShapeDtypeStruct(resid.shape, jnp.bfloat16),
+        scratch_shapes=[pltpu.VMEM((resid.shape[0], returned.shape[0]), jnp.bfloat16)] * 2,
         name="combine",
     )(slot, gates, resid, returned)
 
@@ -233,25 +246,22 @@
         return lax.ppermute(a, "ep", [(r, r ^ k) for r in range(ranks)])
 
     own = w_in.T
-    shards = [own] + [
-        lax.ppermute(own, "ep", [(r, (r + QUAD * d) % ranks) for r in range(ranks)])
-        for d in range(1, quads)
-    ]
+    near = across(normed, 1)
     far = across(normed, 2)
-    near = across(jnp.concatenate([normed, far], axis=0), 1)
-    tokens = jnp.concatenate([normed, far, near], axis=0)
+    shards = [own]
+    for d in range(1, quads):
+        shards += [lax.ppermute(own, "ep", [(r, (r + QUAD * d) % ranks) for r in range(ranks)])]
+    tokens = jnp.concatenate([normed, near, far, across(far, 1)], axis=0)
     table = jnp.concatenate(shards, axis=0)
     partial = dot_t(tokens, table).astype(jnp.bfloat16)
-    order = (0, 2, 1, 3)
     pieces = [partial[:rows]] + [
-        across(partial[i * rows : (i + 1) * rows], order[i]) for i in range(1, QUAD)
+        across(partial[i * rows : (i + 1) * rows], i) for i in range(1, QUAD)
     ]
     joined = jnp.concatenate(pieces, axis=1)
     total = ranks * shard
     source = jnp.arange(total, dtype=jnp.int32)
     which, offset, inside = source // (quads * shard), source // shard % quads, source % shard
-    k = jnp.where(which == 1, 2, jnp.where(which == 2, 1, which))
-    rank = (me // QUAD - offset) % quads * QUAD + ((me % QUAD) ^ k)
+    rank = (me // QUAD - offset) % quads * QUAD + ((me % QUAD) ^ which)
     target = rank * shard + inside
     turn = (target[:, None] == jnp.arange(total, dtype=jnp.int32)[None, :]).astype(jnp.bfloat16)
     return dot(joined, turn).astype(jnp.bfloat16)
@@ -290,10 +300,9 @@
 
     bar_re, bar_im, drive_re, drive_im = discretize(lam_re, lam_im, log_step, in_re, in_im)
     bar = jnp.stack([bar_re.reshape(-1), bar_im.reshape(-1)])
-    copies = max(1, 128 // entries)
 
     def lined(a):
-        return jnp.tile(a.reshape(groups * width, entries), (1, copies))
+        return a.reshape(groups * width, entries)
 
     capacity = 2 * TOPK * count_dev // experts
     flat = route_ids.reshape(-1)
@@ -302,11 +311,8 @@
     slot = (flat * capacity + before).reshape(count_dev, TOPK)
     lane = jnp.arange(experts * capacity, dtype=jnp.int32)
     dispatch = jnp.any(slot.T[:, None, :] == lane[None, :, None], axis=0).astype(jnp.bfloat16)
-    router = jnp.concatenate([w_group, w_route], axis=1)
-    used = router.shape[1]
-    router = jnp.pad(router, ((0, 0), (0, -used % 128)))
-
-    new_state, resid, outgoing, logits = mixer(
+
+    new_state, resid, outgoing, normed2 = mixer(
         inputs,
         state,
         bar,
@@ -317,7 +323,6 @@
         skip[None, :],
         hidden,
         ffn_gain[None, :],
-        router,
         dispatch,
         w_glu,
         w_out,
@@ -330,15 +335,12 @@
     arranged = received.reshape(experts * capacity, model_width)
     gate = dot(arranged, w_gate[0])
     upper = dot(arranged, w_up[0])
-    inner = (jax.nn.silu(gate) * upper).astype(jnp.bfloat16)
+    inner = lax.optimization_barrier((jax.nn.silu(gate) * upper).astype(jnp.bfloat16))
     result = dot(inner, w_down[0]).astype(jnp.bfloat16)
     returned = lax.all_to_all(
         result.reshape(sources, capacity, model_width), "ep", split_axis=0, concat_axis=0, tiled=True
     )
-    groups_used = w_group.shape[1]
-    gates = route_gates(
-        logits[:, :groups_used], logits[:, groups_used:used], route_ids, experts // EXP_GROUPS
-    )
+    gates = route_gates(dot(normed2, w_group), dot(normed2, w_route), route_ids, experts // EXP_GROUPS)
     hidden_out = combine(slot, gates, resid, returned.reshape(experts * capacity, model_width))
     return (hidden_out, new_state)
 

time: 181 us -> 167 us (0.923)
  local copies, waits for them, and re-layouts: 13.5 us -> 2.96 us
  other arithmetic: 11.8 us -> 8.45 us
  starting transfers between devices: 14.5 us -> 17 us
  matrix products: 11.4 us -> 9.52 us
    another operation x13 -> x1, local copies, waits for them, and re-layouts: 7.58 us -> 0.01 us  [the longest x12 7.57 us: lined(): return jnp.tile(a.reshape(groups * width, entries), (1, copies))]
    concatenate x2 -> x0, other arithmetic: 2.85 us -> none  [the longest x1 2.1 us: project(): near = across(jnp.concatenate([normed, far], axis=0), 1)]
    ppermute x5 -> x6, starting transfers between devices: 4.59 us -> 7.1 us  [across(): return lax.ppermute(a, 'ep', [(r, r ^ k) for r in range(ranks)])]
    ppermute x5 -> x6, waiting for transfers between devices: 10.8 us -> 8.44 us  [across(): return lax.ppermute(a, 'ep', [(r, r ^ k) for r in range(ranks)])]
    dot_general x3 -> x6, matrix products: 8.9 us -> 7.31 us  [dot(): return jnp.dot(a, b, preferred_element_type=jnp.float32)]
  transfers between devices with their start and end apart: 9 -> 10, of which waited for: 4 -> 5; matrix products, arithmetic and copies ran while one was open for 13% -> 7% of each run, Pallas kernels for 0% -> 0%
where the time goes in v2:
time: 167 us; the launch traced here: 166 us
  waiting for transfers between devices  55 us (33%)
  blocking collectives  53.5 us (32%)
  Pallas kernels  18.6 us (11%)
  starting transfers between devices  17 us (10%)
  matrix products  9.52 us (6%)
  other arithmetic  8.45 us (5%)
  local copies, waits for them, and re-layouts  2.96 us (2%)
    all_to_all x1, blocking collectives, on_device(): lax.all_to_all(outgoing.reshape(experts, capacity, model_width), 'ep', sp...  53.5 us
    all_to_all x1, waiting for transfers between devices, on_device(): lax.all_to_all(result.reshape(sources, capacity, model_width), 'ep', spli...  46 us
    pallas_call x1, Pallas kernels, mixer(): pl.pallas_call(functools.partial(mixer_kernel, width=width, entries=entri...  14.3 us
    ppermute x6, waiting for transfers between devices, across(): return lax.ppermute(a, 'ep', [(r, r ^ k) for r in range(ranks)])  8.44 us
    dot_general x6, matrix products, dot(): return jnp.dot(a, b, preferred_element_type=jnp.float32)  7.31 us
    ppermute x6, starting transfers between devices, across(): return lax.ppermute(a, 'ep', [(r, r ^ k) for r in range(ranks)])  7.1 us
    all_to_all x1, starting transfers between devices, on_device(): lax.all_to_all(result.reshape(sources, capacity, model_width), 'ep', spli...  5.17 us
    ppermute x3, starting transfers between devices, project(): lax.ppermute(own, 'ep', [(r, (r + QUAD * d) % ranks) for r in range(ranks)])  4.73 us
  transfers between devices with their start and end apart: 10, of which 5 were waited for; matrix products, arithmetic and copies ran while one was open for 7% of the time, Pallas kernels for 0%

profile of v2, /device:TPU:13, one launch (start us, length us, event | category | flops | bytes accessed | tf_op | source)
XLA Modules:
  0.0 166.1 jit_solution(199110981912832436)
XLA Ops:
  0.6 0.0 copy-start
  0.7 0.2 collective-permute-start.5
  0.9 2.3 %collective-permute-start.4 = (bf16[64,2048]{1,0:T(8,128)(2,1)}, bf16[64,2048]{1,0:T(8,128)(2,1)}, u32[]{:S(2)}, u32[]{:S(2)}) collective-permute-start(bf16[64,2048]{1,0:T(8,128)(2,1)} %bitcast.69), channel_id=1, source_target_pairs={{0,8},{1,9},{2,10},{3,11},{4,12},{5,13},{6,14},{7,15},{8,0},{9,1},... | collective-permute-start | bytes 786440 | tf_op jit(solution)/shard_map/ppermute | solution.py:253
  3.2 2.2 %collective-permute-start.3 = (bf16[64,2048]{1,0:T(8,128)(2,1)}, bf16[64,2048]{1,0:T(8,128)(2,1)}, u32[]{:S(2)}, u32[]{:S(2)}) collective-permute-start(bf16[64,2048]{1,0:T(8,128)(2,1)} %bitcast.70), channel_id=1, source_target_pairs={{0,4},{1,5},{2,6},{3,7},{4,8},{5,9},{6,10},{7,11},{8,12},{9,13},{1... | collective-permute-start | bytes 786440 | tf_op jit(solution)/shard_map/ppermute | solution.py:253
  5.4 1.2 fusion.25
  6.6 1.2 fusion.27
  7.9 0.3 collective-permute-start.1
  8.2 1.8 %collective-permute-start = (bf16[128,2048]{1,0:T(8,128)(2,1)S(1)}, bf16[128,2048]{1,0:T(8,128)(2,1)}, u32[]{:S(2)}, u32[]{:S(2)}) collective-permute-start(bf16[128,2048]{1,0:T(8,128)(2,1)S(1)} %fusion.27), channel_id=1, source_target_pairs={{0,1},{1,0},{2,3},{3,2},{4,5},{5,4},{6,7},{7,6},{8,9},{9,8},{10,11... | collective-permute-start | bytes 1572872 | tf_op jit(solution)/shard_map/ppermute | solution.py:246
  10.0 0.7 broadcast_multiply_fusion.1
  10.7 0.8 copy.52
  11.4 0.1 eq.89
  11.6 0.1 eq.85
  11.7 0.7 exp.18
  12.4 0.1 copy.55
  12.5 0.6 reduce-window.6
  13.1 0.2 slice_reduce_fusion
  13.3 0.1 fusion.46
  13.4 0.1 reduce_sum.48
  13.6 0.1 copy.56
  13.7 0.1 fusion.35
  13.7 0.7 convert_element_type.37.dispatch_ref
  14.4 0.2 fusion.43
  14.7 0.1 stack_reshape.7
  14.7 0.1 stack_reshape.6
  14.9 5.2 %collective-permute-done.1 = bf16[128,2048]{1,0:T(8,128)(2,1)} collective-permute-done((bf16[128,2048]{1,0:T(8,128)(2,1)S(1)}, bf16[128,2048]{1,0:T(8,128)(2,1)}, u32[]{:S(2)}, u32[]{:S(2)}) %collective-permute-start.1) | collective-permute-done | bytes 524320 | tf_op jit(solution)/shard_map/ppermute | solution.py:246
  20.0 2.4 %collective-permute-start.2 = (bf16[128,2048]{1,0:T(8,128)(2,1)}, bf16[128,2048]{1,0:T(8,128)(2,1)S(1)}, u32[]{:S(2)}, u32[]{:S(2)}) collective-permute-start(bf16[128,2048]{1,0:T(8,128)(2,1)} %collective-permute-done.1), channel_id=1, source_target_pairs={{0,1},{1,0},{2,3},{3,2},{4,5},{5,4},{6,7},{7,6},{8,9},{9,8},{10,11... | collective-permute-start | bytes 1572872 | tf_op jit(solution)/shard_map/ppermute | solution.py:246
  22.4 0.6 pad_maximum_fusion.bar_ref
  23.0 2.1 %multiply_add_fusion = (f32[64,64,16]{1,2,0:T(8,128)}, f32[64,64,16]{1,2,0:T(8,128)}) fusion(f32[64,64,16]{1,2,0:T(8,128)S(1)} %copy-done.3, f32[64,64,16]{1,2,0:T(8,128)} %param.29, f32[64,64]{1,0:T(8,128)S(1)} %get-tuple-element.21, f32[64,64]{1,0:T(8,128)S(1)} %get-tuple-element.18), kind=kLoop, calls=%fused_computation.34 | loop fusion | flops 393216 | bytes 1081344 | tf_op jit(solution)/shard_map/add | solution.py:32
  25.2 0.6 collective-permute-done.3
  25.7 2.2 %fusion.21 = bf16[512,256]{0,1:T(8,128)(2,1)S(1)} fusion(bf16[128,2048]{1,0:T(8,128)(2,1)S(1)} %collective-permute-done.2, bf16[128,2048]{1,0:T(8,128)(2,1)} %collective-permute-done.1, bf16[128,2048]{1,0:T(8,128)(2,1)} %collective-permute-done, bf16[128,2048]{1,0:T(8,128)(2,1)S(1)} %fusion.27, bf16[64,2048]{1,0:T(8,128)(2,1)} %collective-permute-done.5, ...), kind=kOutput, calls=%fused_computation.21 | convolution fusion | flops 549584896 | bytes 3407872 | tf_op jit(solution)/shard_map/dot_general | solution.py:46
  28.0 1.4 collective-permute-start.8
  29.4 1.2 collective-permute-start.7
  30.7 1.6 collective-permute-done.8
  32.2 1.7 %collective-permute-done.7 = bf16[128,256]{0,1:T(8,128)(2,1)S(1)} collective-permute-done((bf16[128,256]{0,1:T(8,128)(2,1)S(1)}, bf16[128,256]{0,1:T(8,128)(2,1)S(1)}, u32[]{:S(2)}, u32[]{:S(2)}) %collective-permute-start.7) | collective-permute-done | bytes 65568 | tf_op jit(solution)/shard_map/ppermute | solution.py:246
  34.0 1.7 %fusion.24.u_ref = bf16[128,1024]{1,0:T(8,128)(2,1)} fusion(s32[1024]{0:T(1024)S(1)} %fusion.60, bf16[128,256]{0,1:T(8,128)(2,1)S(1)} %collective-permute-done.8, bf16[128,256]{0,1:T(8,128)(2,1)S(1)} %collective-permute-done.7, bf16[128,256]{0,1:T(8,128)(2,1)S(1)} %collective-permute-done.6, bf16[128,256]{0,1:T(8,128)(2,1)S(1)} %get-tuple-element.14), kind=kOutput, calls=%fused_computation.22 | convolution fusion | flops 270663680 | bytes 528384 | tf_op jit(solution)/shard_map/dot_general | solution.py:42
  35.6 14.3 %mixer.1 = (f32[2,128,4096]{2,1,0:T(8,128)}, bf16[128,2048]{1,0:T(8,128)(2,1)}, bf16[512,2048]{1,0:T(8,128)(2,1)}, bf16[128,2048]{1,0:T(8,128)(2,1)}) custom-call(bf16[128,1024]{1,0:T(8,128)(2,1)} %fusion.24.u_ref, f32[2,128,4096]{2,1,0:T(8,128)} %state_ref.1, f32[2,4096]{1,0:T(2,128)} %pad_maximum_fusion.bar_ref, f32[1024,64]{1,0:T(8,128)} %bitcast.62, ...), custom_call_target="tpu_custom_call" | custom-call | tf_op jit(solution)/shard_map/mixer/pallas_call | solution.py:153
  49.9 53.5 %all_to_all.10 = bf16[16,32,2048]{2,1,0:T(8,128)(2,1)S(1)} all-to-all(bf16[16,32,2048]{2,1,0:T(8,128)(2,1)} %bitcast.58), channel_id=1, replica_groups=mesh['grp'=2,'ep'=16] {'ep'}, dimensions={0} | all-to-all | bytes 4194304 | tf_op jit(solution)/shard_map/all_to_all | solution.py:332
  103.5 1.2 fusion.12
  104.7 0.3 copy-done.10
  105.1 1.3 fusion.18
  106.4 2.6 %convolution_convert_fusion = bf16[512,2048]{1,0:T(8,128)(2,1)} fusion(bf16[512,512]{1,0:T(8,128)(2,1)S(1)} %fusion.18, bf16[1,512,2048]{2,1,0:T(8,128)(2,1)S(1)} %copy-done), kind=kOutput, calls=%fused_computation.2 | convolution fusion | flops 1074790400 | bytes 4718592 | tf_op jit(solution)/shard_map/dot_general | solution.py:42
  109.0 5.2 %all-to-all-start.1 = ((bf16[16,32,2048]{2,1,0:T(8,128)(2,1)}), bf16[16,32,2048]{2,1,0:T(8,128)(2,1)}, u32[]{:S(2)}, u32[]{:S(2)}) async-start(bf16[16,32,2048]{2,1,0:T(8,128)(2,1)} %bitcast.57), calls=%async_computation.1 | async-start | bytes 4194304 | tf_op jit(solution)/shard_map/all_to_all | solution.py:340
  114.2 0.2 fusion.69
  114.5 0.1 copy.58
  114.6 0.3 select_reduce_fusion.1
  114.9 0.7 broadcast_multiply_fusion.gates_ref
  115.6 46.0 %all-to-all-done.1 = bf16[16,32,2048]{2,1,0:T(8,128)(2,1)} async-done(((bf16[16,32,2048]{2,1,0:T(8,128)(2,1)}), bf16[16,32,2048]{2,1,0:T(8,128)(2,1)}, u32[]{:S(2)}, u32[]{:S(2)}) %all-to-all-start.1) | async-done | bytes 2097184 | tf_op jit(solution)/shard_map/all_to_all | solution.py:340
  161.7 4.4 %combine.1 = bf16[128,2048]{1,0:T(8,128)(2,1)} custom-call(s32[128,2]{1,0:T(8,128)} %copy-done.2, f32[128,2]{1,0:T(8,128)} %broadcast_multiply_fusion.gates_ref, bf16[128,2048]{1,0:T(8,128)(2,1)} %get-tuple-element.7.resid_ref, bf16[512,2048]{1,0:T(8,128)(2,1)} %bitcast.18.returned_ref), custom_call_target="tpu_custom_call" | custom-call | tf_op jit(solution)/shard_map/combine/pallas_call | solution.py:211
  (41 shorter events, 0.3 us)
Async XLA Ops:
  0.6 105.8 %copy-start = (bf16[1,512,2048]{2,1,0:T(8,128)(2,1)S(1)}, bf16[1,512,2048]{2,1,0:T(8,128)(2,1)}, u32[]{:S(2)}) copy-start(bf16[1,512,2048]{2,1,0:T(8,128)(2,1)} %param.40) | copy-start | bytes 6291460
  0.6 13.8 %copy-start.5 = (f32[64,64]{1,0:T(8,128)S(1)}, f32[64,64]{1,0:T(8,128)}, u32[]{:S(2)}) copy-start(f32[64,64]{1,0:T(8,128)} %param.26) | copy-start | bytes 49156
  0.7 13.8 %copy-start.6 = (f32[64,64]{1,0:T(8,128)S(1)}, f32[64,64]{1,0:T(8,128)}, u32[]{:S(2)}) copy-start(f32[64,64]{1,0:T(8,128)} %param.25) | copy-start | bytes 49156
  0.7 22.4 %copy-start.3 = (f32[64,64,16]{1,2,0:T(8,128)S(1)}, f32[64,64,16]{1,2,0:T(8,128)}, u32[]{:S(2)}) copy-start(f32[64,64,16]{1,2,0:T(8,128)} %param.28) | copy-start | bytes 786436
  0.7 24.5 %collective-permute-start.5 = (bf16[64,2048]{1,0:T(8,128)(2,1)}, bf16[64,2048]{1,0:T(8,128)(2,1)}, u32[]{:S(2)}, u32[]{:S(2)}) collective-permute-start(bf16[64,2048]{1,0:T(8,128)(2,1)} %bitcast.68), channel_id=1, source_target_pairs={{0,12},{1,13},{2,14},{3,15},{4,0},{5,1},{6,2},{7,3},{8,4},{9,5},{1... | collective-permute-start | bytes 786440 | tf_op jit(solution)/shard_map/ppermute | solution.py:253
  0.9 24.3 %collective-permute-start.4 = (bf16[64,2048]{1,0:T(8,128)(2,1)}, bf16[64,2048]{1,0:T(8,128)(2,1)}, u32[]{:S(2)}, u32[]{:S(2)}) collective-permute-start(bf16[64,2048]{1,0:T(8,128)(2,1)} %bitcast.69), channel_id=1, source_target_pairs={{0,8},{1,9},{2,10},{3,11},{4,12},{5,13},{6,14},{7,15},{8,0},{9,1},... | collective-permute-start | bytes 786440 | tf_op jit(solution)/shard_map/ppermute | solution.py:253
  3.2 22.5 %collective-permute-start.3 = (bf16[64,2048]{1,0:T(8,128)(2,1)}, bf16[64,2048]{1,0:T(8,128)(2,1)}, u32[]{:S(2)}, u32[]{:S(2)}) collective-permute-start(bf16[64,2048]{1,0:T(8,128)(2,1)} %bitcast.70), channel_id=1, source_target_pairs={{0,4},{1,5},{2,6},{3,7},{4,8},{5,9},{6,10},{7,11},{8,12},{9,13},{1... | collective-permute-start | bytes 786440 | tf_op jit(solution)/shard_map/ppermute | solution.py:253
  7.9 12.1 %collective-permute-start.1 = (bf16[128,2048]{1,0:T(8,128)(2,1)S(1)}, bf16[128,2048]{1,0:T(8,128)(2,1)}, u32[]{:S(2)}, u32[]{:S(2)}) collective-permute-start(bf16[128,2048]{1,0:T(8,128)(2,1)S(1)} %fusion.27), channel_id=1, source_target_pairs={{0,2},{1,3},{2,0},{3,1},{4,6},{5,7},{6,4},{7,5},{8,10},{9,11},{10,... | collective-permute-start | bytes 1572872 | tf_op jit(solution)/shard_map/ppermute | solution.py:246
  8.2 17.5 %collective-permute-start = (bf16[128,2048]{1,0:T(8,128)(2,1)S(1)}, bf16[128,2048]{1,0:T(8,128)(2,1)}, u32[]{:S(2)}, u32[]{:S(2)}) collective-permute-start(bf16[128,2048]{1,0:T(8,128)(2,1)S(1)} %fusion.27), channel_id=1, source_target_pairs={{0,1},{1,0},{2,3},{3,2},{4,5},{5,4},{6,7},{7,6},{8,9},{9,8},{10,11... | collective-permute-start | bytes 1572872 | tf_op jit(solution)/shard_map/ppermute | solution.py:246
  13.6 14.4 %copy-start.2 = (s32[128,2]{1,0:T(8,128)}, s32[128,2]{1,0:T(8,128)S(1)}, u32[]{:S(2)}) copy-start(s32[128,2]{1,0:T(8,128)S(1)} %add.94.slot_ref) | copy-start | bytes 3076
  14.9 10.9 %copy-start.11 = (bf16[2048,64]{0,1:T(8,128)(2,1)S(1)}, bf16[2048,64]{0,1:T(8,128)(2,1)}, u32[]{:S(2)}) copy-start(bf16[2048,64]{0,1:T(8,128)(2,1)} %param.24) | copy-start | bytes 786436
  20.0 5.7 %collective-permute-start.2 = (bf16[128,2048]{1,0:T(8,128)(2,1)}, bf16[128,2048]{1,0:T(8,128)(2,1)S(1)}, u32[]{:S(2)}, u32[]{:S(2)}) collective-permute-start(bf16[128,2048]{1,0:T(8,128)(2,1)} %collective-permute-done.1), channel_id=1, source_target_pairs={{0,1},{1,0},{2,3},{3,2},{4,5},{5,4},{6,7},{7,6},{8,9},{9,8},{10,11... | collective-permute-start | bytes 1572872 | tf_op jit(solution)/shard_map/ppermute | solution.py:246
  28.0 4.2 %collective-permute-start.8 = (bf16[128,256]{0,1:T(8,128)(2,1)S(1)}, bf16[128,256]{0,1:T(8,128)(2,1)S(1)}, u32[]{:S(2)}, u32[]{:S(2)}) collective-permute-start(bf16[128,256]{0,1:T(8,128)(2,1)S(1)} %get-tuple-element.15), channel_id=1, source_target_pairs={{0,3},{1,2},{2,1},{3,0},{4,7},{5,6},{6,5},{7,4},{8,11},{9,10},{10,... | collective-permute-start | bytes 196616 | tf_op jit(solution)/shard_map/ppermute | solution.py:246
  29.4 4.5 %collective-permute-start.7 = (bf16[128,256]{0,1:T(8,128)(2,1)S(1)}, bf16[128,256]{0,1:T(8,128)(2,1)S(1)}, u32[]{:S(2)}, u32[]{:S(2)}) collective-permute-start(bf16[128,256]{0,1:T(8,128)(2,1)S(1)} %get-tuple-element.16), channel_id=1, source_target_pairs={{0,2},{1,3},{2,0},{3,1},{4,6},{5,7},{6,4},{7,5},{8,10},{9,11},{10,... | collective-permute-start | bytes 196616 | tf_op jit(solution)/shard_map/ppermute | solution.py:246
  30.6 3.3 %collective-permute-start.6 = (bf16[128,256]{0,1:T(8,128)(2,1)S(1)}, bf16[128,256]{0,1:T(8,128)(2,1)S(1)}, u32[]{:S(2)}, u32[]{:S(2)}) collective-permute-start(bf16[128,256]{0,1:T(8,128)(2,1)S(1)} %get-tuple-element.17), channel_id=1, source_target_pairs={{0,1},{1,0},{2,3},{3,2},{4,5},{5,4},{6,7},{7,6},{8,9},{9,8},{10,11... | collective-permute-start | bytes 196616 | tf_op jit(solution)/shard_map/ppermute | solution.py:246
  49.9 53.6 %copy-start.9 = (bf16[1,2048,512]{2,1,0:T(8,128)(2,1)S(1)}, bf16[1,2048,512]{2,1,0:T(8,128)(2,1)}, u32[]{:S(2)}) copy-start(bf16[1,2048,512]{2,1,0:T(8,128)(2,1)} %param.38) | copy-start | bytes 6291460
  103.5 1.6 copy-start.10
  109.0 5.2 %copy-start.8 = (s32[128,2]{0,1:T(2,128)S(1)}, s32[128,2]{0,1:T(2,128)}, u32[]{:S(2)}) copy-start(s32[128,2]{0,1:T(2,128)} %param.41) | copy-start | bytes 3076
  109.0 5.2 %copy-start.1 = (bf16[128,2048]{1,0:T(8,128)(2,1)S(1)}, bf16[128,2048]{1,0:T(8,128)(2,1)}, u32[]{:S(2)}) copy-start(bf16[128,2048]{1,0:T(8,128)(2,1)} %get-tuple-element.6) | copy-start | bytes 1572868
  109.0 5.2 %copy-start.4 = (bf16[2048,16]{0,1:T(8,128)(2,1)S(1)}, bf16[2048,16]{0,1:T(8,128)(2,1)}, u32[]{:S(2)}) copy-start(bf16[2048,16]{0,1:T(8,128)(2,1)} %param.37) | copy-start | bytes 196612
  109.0 5.6 %copy-start.7 = (bf16[2048,4]{0,1:T(4,128)(2,1)S(1)}, bf16[2048,4]{0,1:T(4,128)(2,1)}, u32[]{:S(2)}) copy-start(bf16[2048,4]{0,1:T(4,128)(2,1)} %param.36) | copy-start | bytes 49156
  109.0 52.7 %all-to-all-start.1 = ((bf16[16,32,2048]{2,1,0:T(8,128)(2,1)}), bf16[16,32,2048]{2,1,0:T(8,128)(2,1)}, u32[]{:S(2)}, u32[]{:S(2)}) async-start(bf16[16,32,2048]{2,1,0:T(8,128)(2,1)} %bitcast.57), calls=%async_computation.1 | async-start | bytes 4194304 | tf_op jit(solution)/shard_map/all_to_all | solution.py:340
